TPU v7x, 32 devices: a whole 2x2x4 slice. The times are simulated.
32 devices in a mesh: sp: 8 (over z, core), tp: 4 (over y, x).
Axes of the slice: x: 2, y: 2, z: 4, core: 2. Of those that a mesh axis runs over, the one named last changes fastest.
Arguments:
- query_major: bfloat16 [1024, 3072], P('sp', 'tp'), may hold values from -256 to 256
- query_minor: bfloat16 [1024, 2048], P('sp', 'tp'), may hold values from -256 to 256
- latent_rows: bfloat16 [1024, 512], P('sp'), may hold values from -6 to 6
- rope_keys: bfloat16 [1024, 64], P('sp'), may hold values from -4 to 4
- key_up_major: bfloat16 [512, 2048], P(None, 'tp'), may hold values from -0.25 to 0.25
- value_up_major: bfloat16 [512, 2048], P(None, 'tp'), may hold values from -0.25 to 0.25
- key_up_minor: bfloat16 [512, 1024], P(None, 'tp'), may hold values from -0.25 to 0.25
- value_up_minor: bfloat16 [512, 1024], P(None, 'tp'), may hold values from -0.25 to 0.25
- out_major: bfloat16 [2048, 2048], P('tp'), may hold values from -0.625 to 0.625
- out_minor: bfloat16 [1024, 2048], P('tp'), may hold values from -0.625 to 0.625
- residual: bfloat16 [1024, 2048], P('sp', 'tp'), may hold values from -4 to 4
- norm_gain: float32 [2048], replicated, may hold values from 0.1 to 1.9
- expert_ids: int32 [1024, 2], P('sp'), may hold values from 0 to 7, all different within a row; in each aligned block of 128 rows (0 to 127, 128 to 255, ...) at most 64 rows name the same one
- expert_weights: float32 [1024, 2], P('sp'), may hold values from 0.2 to 1
- gate_proj: bfloat16 [8, 2048, 4096], P('sp', None, 'tp'), may hold values from -0.125 to 0.125
- up_proj: bfloat16 [8, 2048, 4096], P('sp', None, 'tp'), may hold values from -0.125 to 0.125
- down_proj: bfloat16 [8, 4096, 2048], P('sp', 'tp'), may hold values from -0.125 to 0.125
Outputs:
- mixed: bfloat16 [1024, 2048], P('sp', 'tp')
Inputs may be any that keep to these rules, and one draw needn't show every extreme that they name: `expert_ids`: each row names 2 different experts. In each aligned block of 128 rows (the rows of one index of sp) no expert is named by more than 64 rows, and in some blocks one expert is named by exactly 64 rows.
All inputs are finite; a program needn't handle non-finite values.
Results may differ from a plain program's by a relative error of at most 0.02.
Values may be sent and summed in bfloat16 or wider, within the bound.
A program may use at most 64 MiB of HBM per device.

v0:
```python
import functools

import jax
import jax.numpy as jnp
from jax import lax
from jax.experimental import pallas as pl
from jax.experimental.pallas import tpu as pltpu
from jax.sharding import PartitionSpec as P

NOPE_MAJOR = 128
NOPE_MINOR = 64
TOP = 2
MESH = pl.DeviceIdType.MESH

theta_base = 10000.0
norm_eps = 1e-06


def rotary(values, positions):
    half_width = values.shape[-1] // 2
    inverse_freq = 1.0 / theta_base ** (
        jnp.arange(half_width, dtype=jnp.float32) * (2.0 / values.shape[-1])
    )
    angles = positions.astype(jnp.float32)[:, None] * inverse_freq[None, :]
    view_shape = (angles.shape[0],) + (1,) * (values.ndim - 2) + (half_width,)
    cosine = jnp.cos(angles).reshape(view_shape)
    sine_table = jnp.sin(angles).reshape(view_shape)
    lower_half = values[..., :half_width].astype(jnp.float32)
    upper_half = values[..., half_width:].astype(jnp.float32)
    return jnp.concatenate(
        [
            lower_half * cosine - upper_half * sine_table,
            upper_half * cosine + lower_half * sine_table,
        ],
        axis=-1,
    )


def slot_ids(route_block, experts, capacity):
    pairs = route_block.reshape(-1)
    matches = pairs[:, None] == jnp.arange(experts, dtype=jnp.int32)[None, :]
    order = jnp.arange(pairs.shape[0], dtype=jnp.int32)
    earlier = (order[:, None] > order[None, :]).astype(jnp.bfloat16)
    ranks = jnp.dot(earlier, matches.astype(jnp.bfloat16), preferred_element_type=jnp.float32)
    rank = jnp.sum(jnp.where(matches, ranks, 0.0), axis=1).astype(jnp.int32)
    return (pairs * capacity + rank).reshape(route_block.shape)


def remote(src, dst, send_sem, recv_sem, sp_id, tp_id):
    return pltpu.make_async_remote_copy(
        src_ref=src,
        dst_ref=dst,
        send_sem=send_sem,
        recv_sem=recv_sem,
        device_id=(sp_id, tp_id),
        device_id_type=MESH,
    )


def greet(partners):
    barrier = pltpu.get_barrier_semaphore()
    for sp_id, tp_id in partners:
        pl.semaphore_signal(barrier, inc=1, device_id=(sp_id, tp_id), device_id_type=MESH)
    pl.semaphore_wait(barrier, len(partners))


def comm_call(body, out_shape, scratch, collective_id, operands, limit=60 * 1024 * 1024):
    return pl.pallas_call(
        body,
        out_shape=out_shape,
        in_specs=[pl.BlockSpec(memory_space=pltpu.VMEM)] * len(operands),
        out_specs=pl.BlockSpec(memory_space=pltpu.VMEM),
        scratch_shapes=scratch,
        compiler_params=pltpu.CompilerParams(
            collective_id=collective_id, has_side_effects=True, vmem_limit_bytes=limit
        ),
    )(*operands)


def gather_kernel(sp, x_ref, out_ref, up_send, up_recv, side_send, side_recv):
    rows = x_ref.shape[0]
    chips = sp // 2
    sp_id, tp_id = lax.axis_index("sp"), lax.axis_index("tp")
    level, core = sp_id // 2, lax.rem(sp_id, 2)
    sibling = 2 * level + 1 - core
    barrier = pltpu.get_barrier_semaphore()
    pl.semaphore_signal(barrier, inc=1, device_id=(sibling, tp_id), device_id_type=MESH)

    @pl.when(level > 0)
    def _():
        pl.semaphore_signal(barrier, inc=1, device_id=(sp_id - 2, tp_id), device_id_type=MESH)

    @pl.when(level < chips - 1)
    def _():
        pl.semaphore_signal(barrier, inc=1, device_id=(sp_id + 2, tp_id), device_id_type=MESH)

    pl.semaphore_wait(barrier, 1 + lax.min(level, 1) + lax.min(chips - 1 - level, 1))

    def rows_of(index):
        return pl.ds(pl.multiple_of(index * rows, rows), rows)

    def up_copy(step, src):
        place = out_ref.at[rows_of(sp_id - 2 * step), :]
        return remote(src if src is not None else place, place, up_send.at[step], up_recv.at[step], sp_id + 2, tp_id)

    def side_copy(step, src):
        place = out_ref.at[rows_of(sp_id - 2 * step), :]
        return remote(src if src is not None else place, place, side_send.at[step], side_recv.at[step], sibling, tp_id)

    def arrival(sem, index):
        place = out_ref.at[rows_of(index), :]
        return pltpu.make_async_copy(place, place, sem)

    @pl.when(level < chips - 1)
    def _():
        up_copy(0, x_ref).start()

    side_copy(0, x_ref).start()
    out_ref[rows_of(sp_id), :] = x_ref[...]
    for other in range(1, chips):

        @pl.when(level + other < chips)
        def _():
            first = pl.multiple_of((level + other) * 2 * rows, 2 * rows)
            out_ref[pl.ds(first, 2 * rows), :] = jnp.zeros((2 * rows, out_ref.shape[1]), out_ref.dtype)

    for step in range(1, chips):

        @pl.when(level - step >= 0)
        def _():
            arrival(up_recv.at[step - 1], sp_id - 2 * step).wait()

            @pl.when(level < chips - 1)
            def _():
                up_copy(step, None).start()

            side_copy(step, None).start()

    for step in range(chips):

        @pl.when(level - step >= 0)
        def _():
            arrival(side_recv.at[step], sibling - 2 * step).wait()
            side_copy(step, x_ref if step == 0 else None).wait_send()

            @pl.when(level < chips - 1)
            def _():
                up_copy(step, x_ref if step == 0 else None).wait_send()


def reduce_kernel(tp, part_ref, res_ref, out_ref, landed, send_sem, recv_sem):
    width = res_ref.shape[1]
    sp_id, tp_id = lax.axis_index("sp"), lax.axis_index("tp")
    peers = [lax.rem(tp_id + d, tp) for d in range(1, tp)]
    greet([(sp_id, p) for p in peers])

    def columns(index):
        return pl.ds(pl.multiple_of(index * width, width), width)

    copies = []
    for d in range(1, tp):
        copy = remote(
            part_ref.at[:, columns(peers[d - 1])],
            landed.at[d - 1],
            send_sem.at[d - 1],
            recv_sem.at[d - 1],
            sp_id,
            peers[d - 1],
        )
        copy.start()
        copies.append(copy)
    total = part_ref[:, columns(tp_id)].astype(jnp.float32)
    for d in range(1, tp):
        copies[d - 1].wait()
        total = total + landed[d - 1].astype(jnp.float32)
    out_ref[...] = (res_ref[...].astype(jnp.float32) + total).astype(jnp.bfloat16)


def near_first(count):
    order = [0]
    for d in range(1, count // 2 + 1):
        order.append(d)
        if count - d != d:
            order.append(count - d)
    return order


def square(tp_id):
    low = lax.rem(tp_id, 2)
    high = tp_id // 2
    return 2 * high + 1 - low, 2 * (1 - high) + low, 2 * (1 - high) + 1 - low


def dispatch_kernel(sp, tp, x_ref, out_ref, z_send, z_recv, t_send, t_recv, own_sem):
    cap = x_ref.shape[0] // sp
    width = x_ref.shape[1]
    half = cap // 2
    sp_id, tp_id = lax.axis_index("sp"), lax.axis_index("tp")
    greet(
        [(lax.rem(sp_id + d, sp), tp_id) for d in range(1, sp)]
        + [(sp_id, lax.rem(tp_id + d, tp)) for d in range(1, tp)]
    )

    def place(source, owner, part=None):
        first = source * cap
        if part is not None:
            first = first + part * half
        count = cap if part is None else half
        return out_ref.at[
            pl.ds(pl.multiple_of(first, half), count),
            pl.ds(pl.multiple_of(owner * width, width), width),
        ]

    def rows(source, part=None):
        first = source * cap
        if part is not None:
            first = first + part * half
        return x_ref.at[pl.ds(pl.multiple_of(first, half), cap if part is None else half), :]

    order = near_first(sp)
    z_copies = {}
    for d in order[1:]:
        target = lax.rem(sp_id + d, sp)
        z_copies[d] = remote(rows(target), place(sp_id, tp_id), z_send.at[d], z_recv.at[d], target, tp_id)
        z_copies[d].start()
    own = pltpu.make_async_copy(rows(sp_id), place(sp_id, tp_id), own_sem)
    own.start()

    def source_of(d):
        return lax.rem(sp_id + sp - d, sp)

    started = []
    if tp == 4:
        near, far, across = square(tp_id)

        def send(d, part, target, slot, owner):
            copy = remote(
                place(source_of(d), owner, part),
                place(source_of(d), owner, part),
                t_send.at[d, slot],
                t_recv.at[d, slot],
                sp_id,
                target,
            )
            copy.start()
            started.append(copy)
            return copy

        def relay(entry):
            d, to_near, to_far = entry
            to_near[0].wait_recv()
            fourth = send(d, 0, far, 4, near)
            to_far[1].wait_recv()
            fifth = send(d, 1, near, 5, far)
            return [to_near[1], to_far[0], fourth, fifth]

        waiting, rest = None, []
        for d in order:
            if d == 0:
                own.wait()
            else:
                z_copies[d].wait_recv()
            to_near = [send(d, 0, near, 0, tp_id), None]
            to_far = [None, send(d, 1, far, 3, tp_id)]
            to_near[1] = send(d, 1, near, 1, tp_id)
            to_far[0] = send(d, 0, far, 2, tp_id)
            if waiting is not None:
                rest += relay(waiting)
            waiting = (d, to_near, to_far)
        rest += relay(waiting)
        for copy in rest:
            copy.wait_recv()
    else:
        for d in order:
            if d == 0:
                own.wait()
            else:
                z_copies[d].wait_recv()
            for t in range(1, tp):
                copy = remote(
                    place(source_of(d), tp_id),
                    place(source_of(d), tp_id),
                    t_send.at[d, t],
                    t_recv.at[d, t],
                    sp_id,
                    lax.rem(tp_id + t, tp),
                )
                copy.start()
                started.append(copy)
        for copy in started:
            copy.wait_recv()
    for copy in started:
        copy.wait_send()
    for d in order[1:]:
        z_copies[d].wait_send()


def return_kernel(sp, tp, x_ref, out_ref, landed, turned, summed, t_send, t_recv, z_send, z_recv):
    cap = x_ref.shape[0] // sp
    width = out_ref.shape[1]
    half = cap // 2
    sp_id, tp_id = lax.axis_index("sp"), lax.axis_index("tp")
    greet(
        [(lax.rem(sp_id + d, sp), tp_id) for d in range(1, sp)]
        + [(sp_id, lax.rem(tp_id + d, tp)) for d in range(1, tp)]
    )

    def rows_at(target, part=None):
        first = target * cap
        if part is not None:
            first = first + part * half
        return pl.ds(pl.multiple_of(first, half), cap if part is None else half)

    def columns(owner):
        return pl.ds(pl.multiple_of(owner * width, width), width)

    order = near_first(sp)[::-1]
    started, z_copies = [], []

    def push(src, dst, d, slot, target):
        copy = remote(src, dst, t_send.at[d, slot], t_recv.at[d, slot], sp_id, target)
        copy.start()
        started.append(copy)
        return copy

    def deliver(d, target):
        if d == 0:
            return
        copy = remote(
            summed.at[d], out_ref.at[rows_at(sp_id), :], z_send.at[d], z_recv.at[d], target, tp_id
        )
        copy.start()
        z_copies.append(copy)

    def f32(value):
        return value.astype(jnp.float32)

    def place_sum(d, part, value):
        piece = pl.ds(part * half, half)
        summed[d, piece, :] = value.astype(jnp.bfloat16)
        if d == 0:
            out_ref[rows_at(sp_id, part), :] = value.astype(jnp.bfloat16)

    targets = {d: lax.rem(sp_id + d, sp) for d in order}
    if tp == 4:
        near, far, across = square(tp_id)
        first = {}

        def open_block(d):
            target = targets[d]
            first[d] = [
                push(x_ref.at[rows_at(target, 0), columns(across)], landed.at[d, 1], d, 1, near),
                push(x_ref.at[rows_at(target, 1), columns(across)], landed.at[d, 3], d, 3, far),
                push(x_ref.at[rows_at(target, 0), columns(near)], landed.at[d, 0], d, 0, near),
                push(x_ref.at[rows_at(target, 1), columns(far)], landed.at[d, 2], d, 2, far),
            ]

        second = {}

        def turn_block(d):
            target = targets[d]
            first[d][0].wait_recv()
            turned[d, 0] = (f32(x_ref[rows_at(target, 0), columns(far)]) + f32(landed[d, 1])).astype(jnp.bfloat16)
            first[d][1].wait_recv()
            turned[d, 1] = (f32(x_ref[rows_at(target, 1), columns(near)]) + f32(landed[d, 3])).astype(jnp.bfloat16)
            second[d] = [
                push(turned.at[d, 0], landed.at[d, 4], d, 4, far),
                push(turned.at[d, 1], landed.at[d, 5], d, 5, near),
            ]

        def close_block(d):
            target = targets[d]
            first[d][2].wait_recv()
            second[d][0].wait_recv()
            place_sum(d, 0, f32(x_ref[rows_at(target, 0), columns(tp_id)]) + f32(landed[d, 0]) + f32(landed[d, 4]))
            first[d][3].wait_recv()
            second[d][1].wait_recv()
            place_sum(d, 1, f32(x_ref[rows_at(target, 1), columns(tp_id)]) + f32(landed[d, 2]) + f32(landed[d, 5]))
            deliver(d, target)

        count = len(order)
        for i in range(count + 2):
            if i < count:
                open_block(order[i])
            if 0 <= i - 1 < count:
                turn_block(order[i - 1])
            if 0 <= i - 2 < count:
                close_block(order[i - 2])
    else:
        pushed = {}
        for d in order:
            pushed[d] = []
            for t in range(1, tp):
                owner = lax.rem(tp_id + t, tp)
                for part in range(2):
                    slot = 2 * (t - 1) + part
                    pushed[d].append(
                        push(x_ref.at[rows_at(targets[d], part), columns(owner)], landed.at[d, slot], d, slot, owner)
                    )
        for d in order:
            for part in range(2):
                value = f32(x_ref[rows_at(targets[d], part), columns(tp_id)])
                for t in range(1, tp):
                    pushed[d][2 * (t - 1) + part].wait_recv()
                    value = value + f32(landed[d, 2 * (t - 1) + part])
                place_sum(d, part, value)
            deliver(d, targets[d])
    for copy in started:
        copy.wait_send()
    for copy in z_copies:
        copy.wait()


def attention_kernel(
    groups,
    start_ref,
    joined_ref,
    nope_ref,
    rope_ref,
    key_major_ref,
    value_major_ref,
    key_minor_ref,
    value_minor_ref,
    out_major_ref,
    out_minor_ref,
    key_a,
    value_a,
    key_b,
    value_b,
):
    latent = key_major_ref.shape[0]
    tok_rows = nope_ref.shape[1]
    rows_f = joined_ref[:, :latent]
    tail = joined_ref[:, latent:]
    for kept, weight in (
        (key_a, key_major_ref),
        (value_a, value_major_ref),
        (key_b, key_minor_ref),
        (value_b, value_minor_ref),
    ):
        kept[...] = jnp.dot(rows_f, weight[...], preferred_element_type=jnp.float32).astype(jnp.bfloat16)
    total_keys = joined_ref.shape[0]
    shape = (tok_rows, total_keys)
    visible = lax.broadcasted_iota(jnp.int32, shape, 1) <= start_ref[0] + lax.broadcasted_iota(jnp.int32, shape, 0)
    contract = (((1,), (1,)), ((), ()))
    index = 0
    for kept_key, kept_value, out_ref, heads, pack, scale in (
        (key_a, value_a, out_major_ref, *groups[0]),
        (key_b, value_b, out_minor_ref, *groups[1]),
    ):
        tile = kept_key.shape[1] // (-(-heads // pack))
        lanes = lax.broadcasted_iota(jnp.int32, (tok_rows, tile), 1)
        for first in range(0, heads, pack):
            columns = pl.ds(first // pack * tile, tile)
            result = None
            for member in range(min(pack, heads - first)):
                scores = lax.dot_general(
                    nope_ref[index], kept_key[:, columns], contract, preferred_element_type=jnp.float32
                ) + lax.dot_general(rope_ref[index], tail, contract, preferred_element_type=jnp.float32)
                scores = jnp.where(visible, scores * scale, -jnp.inf)
                weights = jnp.exp(scores - jnp.max(scores, axis=1, keepdims=True))
                totals = jnp.sum(weights, axis=1, keepdims=True)
                summed = jnp.dot(
                    weights.astype(jnp.bfloat16), kept_value[:, columns], preferred_element_type=jnp.float32
                ) / totals
                result = summed if result is None else jnp.where(lanes < member * (tile // pack), result, summed)
                index += 1
            out_ref[:, columns] = result.astype(jnp.bfloat16)


def expert_kernel(x_ref, gain_ref, gate_ref, up_ref, down_ref, out_ref, normed, total):
    step = pl.program_id(0)

    @pl.when(step == 0)
    def _():
        rows_f = x_ref[...].astype(jnp.float32)
        power = jnp.mean(rows_f * rows_f, axis=1, keepdims=True)
        normed[...] = (rows_f * lax.rsqrt(power + norm_eps) * gain_ref[...]).astype(jnp.bfloat16)

    rows = normed[...]
    gate_pre = jnp.dot(rows, gate_ref[0], preferred_element_type=jnp.float32)
    up_pre = jnp.dot(rows, up_ref[0], preferred_element_type=jnp.float32)
    hidden = (gate_pre / (1.0 + jnp.exp(-gate_pre)) * up_pre).astype(jnp.bfloat16)
    part = jnp.dot(hidden, down_ref[0], preferred_element_type=jnp.float32)
    last = pl.num_programs(0) - 1

    @pl.when((step == 0) & (last > 0))
    def _():
        total[...] = part

    @pl.when((step > 0) & (step < last))
    def _():
        total[...] += part

    @pl.when((step == last) & (last > 0))
    def _():
        out_ref[...] = (total[...] + part).astype(jnp.bfloat16)

    @pl.when(last == 0)
    def _():
        out_ref[...] = part.astype(jnp.bfloat16)


def run_experts(rows, gain, gate_proj, up_proj, down_proj):
    slots, features = rows.shape
    units = gate_proj.shape[2]
    tile = min(256, units)
    return pl.pallas_call(
        expert_kernel,
        grid=(units // tile,),
        out_shape=jax.ShapeDtypeStruct((slots, features), jnp.bfloat16),
        in_specs=[
            pl.BlockSpec((slots, features), lambda i: (0, 0)),
            pl.BlockSpec((1, features), lambda i: (0, 0)),
            pl.BlockSpec((1, features, tile), lambda i: (0, 0, i)),
            pl.BlockSpec((1, features, tile), lambda i: (0, 0, i)),
            pl.BlockSpec((1, tile, features), lambda i: (0, i, 0)),
        ],
        out_specs=pl.BlockSpec((slots, features), lambda i: (0, 0)),
        scratch_shapes=[
            pltpu.VMEM((slots, features), jnp.bfloat16),
            pltpu.VMEM((slots, features), jnp.float32),
        ],
        compiler_params=pltpu.CompilerParams(vmem_limit_bytes=60 * 1024 * 1024),
    )(rows, gain.reshape(1, -1), gate_proj, up_proj, down_proj)


def pad_columns(array, multiple):
    return jnp.pad(array, ((0, 0), (0, -array.shape[1] % multiple)))


def per_device(
    sp,
    tp,
    query_major,
    query_minor,
    latent_rows,
    rope_keys,
    key_up_major,
    value_up_major,
    key_up_minor,
    value_up_minor,
    out_major,
    out_minor,
    residual,
    norm_gain,
    expert_ids,
    expert_weights,
    gate_proj,
    up_proj,
    down_proj,
):
    tok_rows = query_major.shape[0]
    row_start = lax.axis_index("sp") * tok_rows
    positions = row_start + jnp.arange(tok_rows, dtype=jnp.int32)
    rope_width = rope_keys.shape[1]
    latent = latent_rows.shape[1]
    rope_rot = rotary(rope_keys, positions).astype(jnp.bfloat16)
    heads_major = key_up_major.shape[1] // NOPE_MAJOR
    heads_minor = key_up_minor.shape[1] // NOPE_MINOR
    shaped_major = query_major.reshape(tok_rows, heads_major, NOPE_MAJOR + rope_width)
    shaped_minor = query_minor.reshape(tok_rows, heads_minor, NOPE_MINOR + rope_width)
    nope_major = shaped_major[:, :, :NOPE_MAJOR]
    nope_minor = shaped_minor[:, :, :NOPE_MINOR]
    turned_major = rotary(shaped_major[:, :, NOPE_MAJOR:], positions).astype(jnp.bfloat16)
    turned_minor = rotary(shaped_minor[:, :, NOPE_MINOR:], positions).astype(jnp.bfloat16)
    scale_major = (NOPE_MAJOR + rope_width) ** (-0.5)
    scale_minor = (NOPE_MINOR + rope_width) ** (-0.5)

    joined = jnp.concatenate(
        [latent_rows, rope_rot, jnp.zeros((tok_rows, -(latent + rope_width) % 128), jnp.bfloat16)], axis=1
    )
    dma = pltpu.SemaphoreType.DMA
    chips = sp // 2
    gathered = comm_call(
        functools.partial(gather_kernel, sp),
        jax.ShapeDtypeStruct((sp * tok_rows, joined.shape[1]), jnp.bfloat16),
        [dma((chips,)), dma((chips,)), dma((chips,)), dma((chips,))],
        0,
        (joined,),
    )
    tail_width = joined.shape[1] - latent

    def by_head(array, width):
        return jnp.pad(array.transpose(1, 0, 2), ((0, 0), (0, 0), (0, width - array.shape[2])))

    pack = 128 // NOPE_MINOR
    spread = nope_minor.transpose(1, 0, 2)
    member = (jnp.arange(heads_minor, dtype=jnp.int32) % pack)[:, None, None]
    spread = jnp.concatenate(
        [jnp.where(member == m, spread, jnp.zeros_like(spread)) for m in range(pack)], axis=2
    )
    nope_all = jnp.concatenate([by_head(nope_major, 128), spread], axis=0)
    rope_all = jnp.concatenate([by_head(turned_major, tail_width), by_head(turned_minor, tail_width)], axis=0)
    minor_weights = [pad_columns(key_up_minor, 128), pad_columns(value_up_minor, 128)]
    minor_width = minor_weights[0].shape[1]
    keys = sp * tok_rows
    vmem = pl.BlockSpec(memory_space=pltpu.VMEM)
    attn_major, attn_minor = pl.pallas_call(
        functools.partial(attention_kernel, ((heads_major, 1, scale_major), (heads_minor, pack, scale_minor))),
        out_shape=(
            jax.ShapeDtypeStruct((tok_rows, value_up_major.shape[1]), jnp.bfloat16),
            jax.ShapeDtypeStruct((tok_rows, minor_width), jnp.bfloat16),
        ),
        in_specs=[pl.BlockSpec(memory_space=pltpu.SMEM)] + [vmem] * 7,
        out_specs=(vmem, vmem),
        scratch_shapes=[
            pltpu.VMEM((keys, key_up_major.shape[1]), jnp.bfloat16),
            pltpu.VMEM((keys, value_up_major.shape[1]), jnp.bfloat16),
            pltpu.VMEM((keys, minor_width), jnp.bfloat16),
            pltpu.VMEM((keys, minor_width), jnp.bfloat16),
        ],
        compiler_params=pltpu.CompilerParams(vmem_limit_bytes=60 * 1024 * 1024),
    )(
        row_start.reshape(1).astype(jnp.int32),
        gathered,
        nope_all,
        rope_all,
        key_up_major,
        value_up_major,
        *minor_weights,
    )
    attn_minor = attn_minor[:, : value_up_minor.shape[1]]
    partial_value = jnp.dot(attn_major, out_major, preferred_element_type=jnp.float32)
    partial_value = partial_value + jnp.dot(
        attn_minor, out_minor, preferred_element_type=jnp.float32
    )
    width = residual.shape[1]
    stream_mid = comm_call(
        functools.partial(reduce_kernel, tp),
        jax.ShapeDtypeStruct((tok_rows, width), jnp.bfloat16),
        [pltpu.VMEM((tp - 1, tok_rows, width), jnp.bfloat16), dma((tp - 1,)), dma((tp - 1,))],
        1,
        (partial_value.astype(jnp.bfloat16), residual),
    )
    experts = sp
    capacity = 2 * tok_rows * TOP // experts
    slots = experts * capacity
    slot_list = slot_ids(expert_ids, experts, capacity)
    slot_numbers = jnp.arange(slots, dtype=jnp.int32)
    by_slot = slot_list.T
    select = (slot_numbers[:, None] == by_slot[0][None, :]).astype(jnp.bfloat16)
    for j in range(1, TOP):
        select = select + (slot_numbers[:, None] == by_slot[j][None, :]).astype(jnp.bfloat16)
    placed = jnp.dot(select, stream_mid, preferred_element_type=jnp.float32).astype(jnp.bfloat16)
    slots_t = 6 if tp == 4 else tp
    arrived = comm_call(
        functools.partial(dispatch_kernel, sp, tp),
        jax.ShapeDtypeStruct((slots, tp * width), jnp.bfloat16),
        [dma((sp,)), dma((sp,)), dma((sp, slots_t)), dma((sp, slots_t)), dma],
        2,
        (placed,),
    )
    down_part = run_experts(arrived, norm_gain, gate_proj, up_proj, down_proj)
    pieces = 6 if tp == 4 else 2 * (tp - 1)
    half = capacity // 2
    flat_out = comm_call(
        functools.partial(return_kernel, sp, tp),
        jax.ShapeDtypeStruct((slots, width), jnp.bfloat16),
        [
            pltpu.VMEM((sp, pieces, half, width), jnp.bfloat16),
            pltpu.VMEM((sp, 2, half, width), jnp.bfloat16),
            pltpu.VMEM((sp, capacity, width), jnp.bfloat16),
            dma((sp, pieces)),
            dma((sp, pieces)),
            dma((sp,)),
            dma((sp,)),
        ],
        3,
        (down_part,),
    )
    mixed = stream_mid.astype(jnp.float32)
    for j in range(TOP):
        hot = (slot_list[:, j : j + 1] == slot_numbers[None, :]).astype(jnp.bfloat16)
        mixed = mixed + jnp.dot(hot, flat_out, preferred_element_type=jnp.float32) * expert_weights[:, j : j + 1]
    return mixed.astype(jnp.bfloat16)


def solution(mesh):
    in_specs = (
        P("sp", "tp"),
        P("sp", "tp"),
        P("sp", None),
        P("sp", None),
        P(None, "tp"),
        P(None, "tp"),
        P(None, "tp"),
        P(None, "tp"),
        P("tp", None),
        P("tp", None),
        P("sp", "tp"),
        P(),
        P("sp", None),
        P("sp", None),
        P("sp", None, "tp"),
        P("sp", None, "tp"),
        P("sp", "tp", None),
    )
    out_specs = P("sp", "tp")
    return jax.shard_map(
        functools.partial(per_device, mesh.shape["sp"], mesh.shape["tp"]),
        mesh=mesh,
        in_specs=in_specs,
        out_specs=out_specs,
        check_vma=False,
    )
```

profile of v0, /device:TPU:0, one launch (start us, length us, event | category | flops | bytes accessed | tf_op | source)
XLA Modules:
  0.0 122.7 jit_solution(5605428195321497822)
XLA Ops:
  0.0 0.0 copy-start
  0.0 0.9 slice_convert_fusion.2
  0.9 0.1 copy.46
  1.0 0.1 copy.61
  1.1 1.0 multiply_cosine_fusion
  2.1 1.1 copy.49
  3.2 0.0 copy-start.3
  3.2 0.1 copy.53
  3.3 1.0 copy.51
  4.4 0.1 copy.56
  4.5 0.1 copy.64
  4.6 0.1 copy.65
  4.8 0.0 copy-start.4
  4.8 0.2 fusion.8
  5.0 0.1 maximum_bitcast_fusion
  5.1 0.8 fusion.15.rope_ref
  5.9 0.1 pad.21.clone
  5.9 0.0 copy-done.3
  6.0 0.0 copy-done.4
  6.0 0.8 maximum_maximum_fusion.1.x_ref
  6.7 8.6 %shard_map.163.joined_ref = bf16[1024,640]{1,0:T(8,128)(2,1)} custom-call(bf16[128,640]{1,0:T(8,128)(2,1)} %maximum_maximum_fusion.1.x_ref), custom_call_target="tpu_custom_call" | custom-call | tf_op jit(solution)/shard_map/pallas_call | solution.py:68
  15.4 0.1 copy.63
  15.5 0.1 select_bitcast_fusion.1
  15.6 0.1 copy.62
  15.8 0.0 copy-start.2
  15.8 0.8 maximum_maximum_fusion.nope_ref
  16.6 7.7 %shard_map.164 = (bf16[128,512]{1,0:T(8,128)(2,1)}, bf16[128,256]{1,0:T(8,128)(2,1)}) custom-call(s32[1]{0:T(128)} %bitcast.start_ref, bf16[1024,640]{1,0:T(8,128)(2,1)} %shard_map.163.joined_ref, bf16[8,128,128]{2,1,0:T(8,128)(2,1)} %maximum_maximum_fusion.nope_ref, bf16[8,128,128]{2,1,0:T(8,128)(2,1)} %fusion.15.rope_ref, bf16[512,512]{1,0:T(8,128)(2,1)} %key_major_ref.1, ...), custom_call_target="tpu_custom_call" | custom-call | tf_op jit(solution)/shard_map/pallas_call | solution.py:599
  24.3 0.0 copy-start.5
  24.3 0.0 copy-done.2
  24.3 1.2 fusion.30
  25.5 0.0 copy-done
  25.5 0.0 copy-done.5
  25.5 0.0 copy-start.6
  25.5 1.2 %fusion.part_ref = bf16[128,2048]{1,0:T(8,128)(2,1)} fusion(f32[128,2048]{1,0:T(8,128)S(1)} %fusion.30, bf16[128,512]{1,0:T(8,128)(2,1)S(1)} %copy-done.5, bf16[512,2048]{1,0:T(8,128)(2,1)S(1)} %copy-done), kind=kOutput, calls=%fused_computation.1 | convolution fusion | flops 268959744 | bytes 3801088 | tf_op jit(solution)/shard_map/dot_general | solution.py:624
  26.8 10.0 %shard_map.165 = bf16[128,512]{1,0:T(8,128)(2,1)} custom-call(bf16[128,2048]{1,0:T(8,128)(2,1)} %fusion.part_ref, bf16[128,512]{1,0:T(8,128)(2,1)} %res_ref.1), custom_call_target="tpu_custom_call" | custom-call | tf_op jit(solution)/shard_map/pallas_call | solution.py:68
  36.8 0.0 copy-done.6
  36.8 0.1 copy.59
  36.9 0.1 eq.95
  37.0 0.2 fusion.4
  37.2 0.1 convert_element_type.72
  37.4 0.1 copy.60
  37.5 2.0 %convolution_convert_fusion.x_ref = bf16[512,512]{1,0:T(8,128)(2,1)} fusion(bf16[128,512]{1,0:T(8,128)(2,1)} %shard_map.165, s32[128]{0:T(128)S(1)} %get-tuple-element.30, s32[128]{0:T(128)S(1)} %get-tuple-element.29), kind=kOutput, calls=%fused_computation.2 | convolution fusion | flops 67895296 | bytes 656384 | tf_op jit(solution)/shard_map/dot_general | solution.py:645
  39.5 39.4 %shard_map.166.x_ref = bf16[512,2048]{1,0:T(8,128)(2,1)} custom-call(bf16[512,512]{1,0:T(8,128)(2,1)} %convolution_convert_fusion.x_ref), custom_call_target="tpu_custom_call" | custom-call | tf_op jit(solution)/shard_map/pallas_call | solution.py:68
  78.9 13.8 %shard_map.167.x_ref = bf16[512,2048]{1,0:T(8,128)(2,1)} custom-call(bf16[512,2048]{1,0:T(8,128)(2,1)} %shard_map.166.x_ref, f32[1,2048]{1,0:T(1,128)} %bitcast.39, bf16[1,2048,1024]{2,1,0:T(8,128)(2,1)} %gate_ref.1, bf16[1,2048,1024]{2,1,0:T(8,128)(2,1)} %up_ref.1, bf16[1,1024,2048]{2,1,0:T(8,128)(2,1)} %down_ref.1), custom_call_target="tpu_custom_call" | custom-call | tf_op jit(solution)/shard_map/pallas_call | solution.py:508
  92.7 0.0 copy-start.7
  92.7 0.0 copy-start.1
  92.7 26.7 %shard_map.168 = bf16[512,512]{1,0:T(8,128)(2,1)} custom-call(bf16[512,2048]{1,0:T(8,128)(2,1)} %shard_map.167.x_ref), custom_call_target="tpu_custom_call" | custom-call | tf_op jit(solution)/shard_map/pallas_call | solution.py:68
  119.4 0.0 copy-done.7
  119.4 0.0 copy-done.1
  119.4 1.3 %fusion.2 = f32[128,512]{1,0:T(8,128)S(1)} fusion(bf16[512,512]{1,0:T(8,128)(2,1)} %shard_map.168, bf16[128,512]{1,0:T(8,128)(2,1)S(1)} %copy-done.1, f32[128]{0:T(128)S(1)} %get-tuple-element.28, s32[128]{0:T(128)S(1)} %get-tuple-element.26), kind=kOutput, calls=%fused_computation.6 | convolution fusion | flops 67371008 | bytes 918528 | tf_op jit(solution)/shard_map/dot_general | solution.py:675
  120.7 2.0 %fusion.3 = bf16[128,512]{1,0:T(8,128)(2,1)} fusion(f32[128,512]{1,0:T(8,128)S(1)} %fusion.2, bf16[512,512]{1,0:T(8,128)(2,1)} %shard_map.168, f32[128]{0:T(128)S(1)} %get-tuple-element.27, s32[128]{0:T(128)S(1)} %get-tuple-element.25), kind=kOutput, calls=%fused_computation.7 | convolution fusion | flops 67371008 | bytes 918528 | tf_op jit(solution)/shard_map/dot_general | solution.py:675
  (13 shorter events, 0.1 us)
Async XLA Ops:
  0.0 25.5 %copy-start = (bf16[512,2048]{1,0:T(8,128)(2,1)S(1)}, bf16[512,2048]{1,0:T(8,128)(2,1)}, u32[]{:S(2)}) copy-start(bf16[512,2048]{1,0:T(8,128)(2,1)} %param.25) | copy-start | bytes 6291460
  3.2 2.8 %copy-start.3 = (bf16[128,512]{1,0:T(8,128)(2,1)S(1)}, bf16[128,512]{1,0:T(8,128)(2,1)}, u32[]{:S(2)}) copy-start(bf16[128,512]{1,0:T(8,128)(2,1)} %param.19) | copy-start | bytes 393220
  4.8 1.2 copy-start.4
  15.8 8.5 %copy-start.2 = (bf16[256,2048]{1,0:T(8,128)(2,1)S(1)}, bf16[256,2048]{1,0:T(8,128)(2,1)}, u32[]{:S(2)}) copy-start(bf16[256,2048]{1,0:T(8,128)(2,1)} %param.26) | copy-start | bytes 3145732
  24.3 1.2 copy-start.5
  25.5 11.3 %copy-start.6 = (s32[128,2]{0,1:T(2,128)S(1)}, s32[128,2]{0,1:T(2,128)}, u32[]{:S(2)}) copy-start(s32[128,2]{0,1:T(2,128)} %param.29) | copy-start | bytes 3076
  92.7 26.7 %copy-start.7 = (f32[128,2]{0,1:T(2,128)S(1)}, f32[128,2]{0,1:T(2,128)}, u32[]{:S(2)}) copy-start(f32[128,2]{0,1:T(2,128)} %param.30) | copy-start | bytes 3076
  92.7 26.7 %copy-start.1 = (bf16[128,512]{1,0:T(8,128)(2,1)S(1)}, bf16[128,512]{1,0:T(8,128)(2,1)}, u32[]{:S(2)}) copy-start(bf16[128,512]{1,0:T(8,128)(2,1)} %shard_map.165) | copy-start | bytes 393220
where the time goes:
time: 123 us
  Pallas kernels  106 us (86%)
  matrix products  7.95 us (6%)
  other arithmetic  4.59 us (4%)
  local copies, waits for them, and re-layouts  3.7 us (3%)
    pallas_call x4, Pallas kernels, comm_call(): pl.pallas_call(body, out_shape=out_shape, in_specs=[pl.BlockSpec(memory_s...  84.7 us
    pallas_call x1, Pallas kernels, run_experts(): pl.pallas_call(expert_kernel, grid=(units // tile,), out_shape=jax.ShapeD...  13.8 us
    pallas_call x1, Pallas kernels, per_device(): pl.pallas_call(functools.partial(attention_kernel, ((heads_major, 1, scal...  7.69 us
    dot_general x2, matrix products, per_device(): jnp.dot(hot, flat_out, preferred_element_type=jnp.float32)  3.3 us
    unnamed x24, local copies, waits for them, and re-layouts  2.9 us

commit v1 on v0

--- a/solution.py
+++ b/solution.py
@@ -501,6 +501,326 @@
         out_ref[...] = part.astype(jnp.bfloat16)
 
 
+def flip(index, offset):
+    step = 1
+    while step <= offset:
+        if offset & step:
+            index = index + step * (1 - 2 * lax.rem(index // step, 2))
+        step *= 2
+    return index
+
+
+def moe_kernel(
+    sp,
+    x_ref,
+    ids_ref,
+    ids_t_ref,
+    mix_ref,
+    gain_ref,
+    gate_ref,
+    up_ref,
+    down_ref,
+    out_ref,
+    gate,
+    up,
+    down,
+    placed,
+    rows_in,
+    normed,
+    hidden,
+    part,
+    landed,
+    turned,
+    summed,
+    returned,
+    hot,
+    load_sem,
+    z_send,
+    z_recv,
+    t_send,
+    t_recv,
+    r_send,
+    r_recv,
+    y_send,
+    y_recv,
+):
+    tok_rows, width = x_ref.shape
+    features = rows_in.shape[2]
+    chips = sp // 2
+    slots = placed.shape[0]
+    cap = slots // sp
+    units = gate.shape[1]
+    sp_id, tp_id = lax.axis_index("sp"), lax.axis_index("tp")
+    near, far, across = square(tp_id)
+
+    loads = []
+    pieces = load_sem.shape[1]
+    for index, (src, dst) in enumerate(((gate_ref, gate), (up_ref, up), (down_ref, down))):
+        rows = dst.shape[0] // pieces
+        for piece in range(pieces):
+            span = pl.ds(piece * rows, rows)
+            copy = pltpu.make_async_copy(src.at[0, span, :], dst.at[span, :], load_sem.at[index, piece])
+            copy.start()
+            loads.append(copy)
+
+    barrier = pltpu.get_barrier_semaphore()
+    for offset in range(1, sp):
+        pl.semaphore_signal(barrier, inc=1, device_id=(flip(sp_id, offset), tp_id), device_id_type=MESH)
+    for peer in (near, far, across):
+        pl.semaphore_signal(barrier, inc=1, device_id=(sp_id, peer), device_id_type=MESH)
+
+    lanes = lax.broadcasted_iota(jnp.int32, (sp, tok_rows), 0)
+    matches_t = [(lanes == ids_t_ref[j : j + 1, :]).astype(jnp.float32) for j in range(TOP)]
+    order = (tok_rows, tok_rows)
+    before_t = (lax.broadcasted_iota(jnp.int32, order, 0) < lax.broadcasted_iota(jnp.int32, order, 1)).astype(
+        jnp.bfloat16
+    )
+    named_t = functools.reduce(lambda a, b: a + b, matches_t)
+    earlier_t = jnp.dot(named_t.astype(jnp.bfloat16), before_t, preferred_element_type=jnp.float32)
+    slot_rows = lax.broadcasted_iota(jnp.int32, (slots, tok_rows), 0)
+    select = None
+    for j in range(TOP):
+        rank = jnp.sum(matches_t[j] * earlier_t, axis=0, keepdims=True).astype(jnp.int32)
+        earlier_t = earlier_t + matches_t[j]
+        chosen = jnp.where(slot_rows == ids_t_ref[j : j + 1, :] * cap + rank, 1.0, 0.0)
+        select = chosen if select is None else select + chosen
+    placed[...] = jnp.dot(select.astype(jnp.bfloat16), x_ref[...], preferred_element_type=jnp.float32).astype(
+        jnp.bfloat16
+    )
+
+    def block(index):
+        return pl.ds(pl.multiple_of(index * cap, cap), cap)
+
+    def columns(owner):
+        return pl.ds(pl.multiple_of(owner * width, width), width)
+
+    own_columns = columns(tp_id)
+    pl.semaphore_wait(barrier, sp - 1 + 3)
+
+    z_copies = {}
+    for offset in range(1, sp):
+        target = flip(sp_id, offset)
+        k, q = offset // 2, offset % 2
+        z_copies[offset] = remote(
+            placed.at[block(target), :],
+            rows_in.at[k, pl.ds(q * cap, cap), own_columns],
+            z_send.at[offset],
+            z_recv.at[offset],
+            target,
+            tp_id,
+        )
+        z_copies[offset].start()
+    rows_in[0, 0:cap, own_columns] = placed[block(sp_id), :]
+
+    started = []
+
+    def pass_on(k, q, owner, slot, target):
+        place = rows_in.at[k, pl.ds(q * cap, cap), columns(owner)]
+        copy = remote(place, place, t_send.at[k, slot], t_recv.at[k, slot], sp_id, target)
+        copy.start()
+        started.append(copy)
+        return copy
+
+    arriving = {}
+
+    def open_chunk(k):
+        if k == 0:
+            first = [pass_on(0, 0, tp_id, 0, near), pass_on(0, 0, tp_id, 2, far)]
+            z_copies[1].wait_recv()
+            second = [pass_on(0, 1, tp_id, 3, far), pass_on(0, 1, tp_id, 1, near)]
+            arriving[0] = [first[0], second[1], first[1], second[0]]
+            return
+        z_copies[2 * k].wait_recv()
+        a = pass_on(k, 0, tp_id, 0, near)
+        z_copies[2 * k + 1].wait_recv()
+        d = pass_on(k, 1, tp_id, 3, far)
+        b = pass_on(k, 1, tp_id, 1, near)
+        c = pass_on(k, 0, tp_id, 2, far)
+        arriving[k] = [a, b, c, d]
+
+    def relay(k):
+        a, b, c, d = arriving[k]
+        a.wait_recv()
+        e = pass_on(k, 0, near, 4, far)
+        d.wait_recv()
+        f = pass_on(k, 1, far, 5, near)
+        arriving[k] = [b, c, e, f]
+
+    def ready(k):
+        for copy in arriving[k]:
+            copy.wait_recv()
+        rows = rows_in[k].astype(jnp.float32)
+        power = jnp.mean(rows * rows, axis=1, keepdims=True)
+        normed[...] = (rows * lax.rsqrt(power + norm_eps) * gain_ref[...]).astype(jnp.bfloat16)
+
+    def expand():
+        tile = 256
+        rows = normed[...]
+        for first in range(0, units, tile):
+            span = slice(first, first + tile)
+            gate_pre = jnp.dot(rows, gate[:, span], preferred_element_type=jnp.float32)
+            up_pre = jnp.dot(rows, up[:, span], preferred_element_type=jnp.float32)
+            hidden[:, span] = (gate_pre / (1.0 + jnp.exp(-gate_pre)) * up_pre).astype(jnp.bfloat16)
+
+    def push(src, dst, k, slot, target):
+        copy = remote(src, dst, r_send.at[k, slot], r_recv.at[k, slot], sp_id, target)
+        copy.start()
+        started.append(copy)
+        return copy
+
+    halves = (pl.ds(0, cap), pl.ds(cap, cap))
+    leaving, turning = {}, {}
+
+    def contract(k):
+        rows = hidden[...]
+
+        def fill(owner):
+            part[k, :, columns(owner)] = jnp.dot(
+                rows, down[:, columns(owner)], preferred_element_type=jnp.float32
+            ).astype(jnp.bfloat16)
+
+        def send(q, owner, slot, target):
+            return push(part.at[k, halves[q], columns(owner)], landed.at[k, slot], k, slot, target)
+
+        fill(across)
+        second = send(0, across, 1, near)
+        fourth = send(1, across, 3, far)
+        fill(near)
+        first = send(0, near, 0, near)
+        fill(far)
+        third = send(1, far, 2, far)
+        fill(tp_id)
+        leaving[k] = [first, second, third, fourth]
+
+    def f32(value):
+        return value.astype(jnp.float32)
+
+    def turn(k):
+        leaving[k][1].wait_recv()
+        turned[k, 0] = (f32(part[k, halves[0], columns(far)]) + f32(landed[k, 1])).astype(jnp.bfloat16)
+        a = push(turned.at[k, 0], landed.at[k, 4], k, 4, far)
+        leaving[k][3].wait_recv()
+        turned[k, 1] = (f32(part[k, halves[1], columns(near)]) + f32(landed[k, 3])).astype(jnp.bfloat16)
+        b = push(turned.at[k, 1], landed.at[k, 5], k, 5, near)
+        turning[k] = [a, b]
+
+    back = {}
+
+    def close(k):
+        for q in range(2):
+            leaving[k][2 * q].wait_recv()
+            turning[k][q].wait_recv()
+            value = f32(part[k, halves[q], own_columns]) + f32(landed[k, 2 * q]) + f32(landed[k, 4 + q])
+            offset = 2 * k + q
+            if offset == 0:
+                returned[block(sp_id), :] = value.astype(jnp.bfloat16)
+                continue
+            summed[k, q] = value.astype(jnp.bfloat16)
+            back[offset] = remote(
+                summed.at[k, q],
+                returned.at[block(sp_id), :],
+                y_send.at[offset],
+                y_recv.at[offset],
+                flip(sp_id, offset),
+                tp_id,
+            )
+            back[offset].start()
+
+    open_chunk(0)
+    relay(0)
+    open_chunk(1)
+    lanes = lax.broadcasted_iota(jnp.int32, (tok_rows, sp), 1)
+    matches = [(lanes == ids_ref[:, j : j + 1]).astype(jnp.float32) for j in range(TOP)]
+    before = (lax.broadcasted_iota(jnp.int32, order, 0) > lax.broadcasted_iota(jnp.int32, order, 1)).astype(
+        jnp.bfloat16
+    )
+    named = functools.reduce(lambda a, b: a + b, matches)
+    earlier = jnp.dot(before, named.astype(jnp.bfloat16), preferred_element_type=jnp.float32)
+    slot_lanes = lax.broadcasted_iota(jnp.int32, (tok_rows, slots), 1)
+    for j in range(TOP):
+        rank = jnp.sum(matches[j] * earlier, axis=1, keepdims=True).astype(jnp.int32)
+        earlier = earlier + matches[j]
+        hot[j] = jnp.where(slot_lanes == ids_ref[:, j : j + 1] * cap + rank, 1.0, 0.0).astype(jnp.bfloat16)
+    for copy in loads:
+        copy.wait()
+    relay(1)
+    if chips > 2:
+        open_chunk(2)
+    turns = list(range(1, chips)) + [0]
+    for index, k in enumerate(turns):
+        ready(k)
+        expand()
+        if index + 2 < chips:
+            relay(index + 2)
+        if index + 3 < chips:
+            open_chunk(index + 3)
+        contract(k)
+        if index >= 1:
+            turn(turns[index - 1])
+        if index >= 2:
+            close(turns[index - 2])
+    turn(turns[-1])
+    close(turns[-2])
+    close(turns[-1])
+    for offset in range(1, sp):
+        back[offset].wait_recv()
+    total = x_ref[...].astype(jnp.float32)
+    for j in range(TOP):
+        total = total + jnp.dot(hot[j], returned[...], preferred_element_type=jnp.float32) * mix_ref[:, j : j + 1]
+    out_ref[...] = total.astype(jnp.bfloat16)
+    for copy in started:
+        copy.wait_send()
+    for offset in range(1, sp):
+        z_copies[offset].wait_send()
+        back[offset].wait_send()
+
+
+def fused_experts(sp, tp, stream_mid, ids, mix, gain, gate_proj, up_proj, down_proj):
+    tok_rows, width = stream_mid.shape
+    cap = 2 * tok_rows * TOP // sp
+    slots = sp * cap
+    chips = sp // 2
+    features = tp * width
+    units = gate_proj.shape[2]
+    dma = pltpu.SemaphoreType.DMA
+    vmem = pl.BlockSpec(memory_space=pltpu.VMEM)
+    hbm = pl.BlockSpec(memory_space=pl.ANY)
+    bf16 = jnp.bfloat16
+    return pl.pallas_call(
+        functools.partial(moe_kernel, sp),
+        out_shape=jax.ShapeDtypeStruct((tok_rows, width), bf16),
+        in_specs=[vmem] * 5 + [hbm] * 3,
+        out_specs=vmem,
+        scratch_shapes=[
+            pltpu.VMEM((features, units), bf16),
+            pltpu.VMEM((features, units), bf16),
+            pltpu.VMEM((units, features), bf16),
+            pltpu.VMEM((slots, width), bf16),
+            pltpu.VMEM((chips, 2 * cap, features), bf16),
+            pltpu.VMEM((2 * cap, features), bf16),
+            pltpu.VMEM((2 * cap, units), bf16),
+            pltpu.VMEM((chips, 2 * cap, features), bf16),
+            pltpu.VMEM((chips, 6, cap, width), bf16),
+            pltpu.VMEM((chips, 2, cap, width), bf16),
+            pltpu.VMEM((chips, 2, cap, width), bf16),
+            pltpu.VMEM((slots, width), bf16),
+            pltpu.VMEM((TOP, tok_rows, slots), bf16),
+            dma((3, 4)),
+            dma((sp,)),
+            dma((sp,)),
+            dma((chips, 6)),
+            dma((chips, 6)),
+            dma((chips, 6)),
+            dma((chips, 6)),
+            dma((sp,)),
+            dma((sp,)),
+        ],
+        compiler_params=pltpu.CompilerParams(
+            collective_id=4, has_side_effects=True, vmem_limit_bytes=60 * 1024 * 1024
+        ),
+    )(stream_mid, ids, ids.T, mix, gain.reshape(1, -1), gate_proj, up_proj, down_proj)
+
+
 def run_experts(rows, gain, gate_proj, up_proj, down_proj):
     slots, features = rows.shape
     units = gate_proj.shape[2]
@@ -633,6 +953,10 @@
         1,
         (partial_value.astype(jnp.bfloat16), residual),
     )
+    if tp == 4 and sp & (sp - 1) == 0 and (2 * tok_rows * TOP // sp) % 16 == 0:
+        return fused_experts(
+            sp, tp, stream_mid, expert_ids, expert_weights, norm_gain, gate_proj, up_proj, down_proj
+        )
     experts = sp
     capacity = 2 * tok_rows * TOP // experts
     slots = experts * capacity

time: 123 us -> 101 us (0.82)
  the two profiles are of different devices: /device:TPU:0 before, /device:TPU:25 now
where the time goes in v1:
time: 101 us; the launch traced here: 99.5 us
  Pallas kernels  85.3 us (84%)
  local copies, waits for them, and re-layouts  6.68 us (7%)
  other arithmetic  4.88 us (5%)
  matrix products  2.44 us (2%)
    pallas_call x1, Pallas kernels, fused_experts(): pl.pallas_call(functools.partial(moe_kernel, sp), out_shape=jax.ShapeDtyp...  49.3 us
    pallas_call x2, Pallas kernels, comm_call(): pl.pallas_call(body, out_shape=out_shape, in_specs=[pl.BlockSpec(memory_s...  28.3 us
    pallas_call x1, Pallas kernels, per_device(): pl.pallas_call(functools.partial(attention_kernel, ((heads_major, 1, scal...  7.7 us
    unnamed x18, local copies, waits for them, and re-layouts  6.23 us

profile of v1, /device:TPU:25, one launch (start us, length us, event | category | flops | bytes accessed | tf_op | source)
XLA Modules:
  0.0 99.5 jit_solution(249889364889046383)
XLA Ops:
  0.0 0.0 copy-start
  0.0 0.0 copy-start.2
  0.1 0.1 pad.21.clone
  0.1 0.9 slice_convert_fusion.2
  1.0 0.1 copy.49
  1.1 0.1 copy.34
  1.2 1.4 %copy.48.mix_ref = f32[128,2]{1,0:T(8,128)} copy(f32[128,2]{0,1:T(2,128)} %param.30) | data formatting | bytes 2048 | tf_op args[13]
  2.6 1.4 %copy.47.ids_ref = s32[128,2]{1,0:T(8,128)} copy(s32[128,2]{0,1:T(2,128)} %param.29) | data formatting | bytes 2048 | tf_op args[12]
  4.0 0.3 multiply_cosine_fusion
  4.4 1.0 %copy.39 = bf16[128,512]{0,1:T(8,128)(2,1)S(1)} copy(bf16[128,512]{1,0:T(8,128)(2,1)} %param.18) | data formatting | bytes 262144 | tf_op args[1]
  5.4 0.1 copy.51
  5.6 0.1 select_bitcast_fusion.1
  5.7 0.1 copy.53
  5.8 1.7 %maximum_maximum_fusion.1.x_ref = bf16[128,640]{1,0:T(8,128)(2,1)} fusion(bf16[128,32]{1,0:T(8,128)(2,1)S(1)} %get-tuple-element.27, bf16[128,32]{1,0:T(8,128)(2,1)S(1)} %get-tuple-element.28, bf16[128,512]{1,0:T(8,128)(2,1)} %param.19, bf16[640]{0:T(1024)(128)(2,1)S(1)} %pad.21.clone), kind=kLoop, calls=%fused_computation.20 | loop fusion | flops 655360 | bytes 312576 | tf_op jit(solution)/shard_map/concatenate | solution.py:890
  7.5 0.1 copy.44
  7.6 0.0 copy-done.2
  7.6 0.2 copy.37
  7.8 0.1 copy.50
  7.9 0.8 maximum_maximum_fusion.nope_ref
  8.8 0.1 copy.52
  8.9 0.1 copy.41
  9.0 0.2 fusion.4
  9.2 0.1 maximum_bitcast_fusion
  9.4 0.8 fusion.11.rope_ref
  10.1 0.0 copy-start.1
  10.1 17.3 %shard_map.163.joined_ref = bf16[1024,640]{1,0:T(8,128)(2,1)} custom-call(bf16[128,640]{1,0:T(8,128)(2,1)} %maximum_maximum_fusion.1.x_ref), custom_call_target="tpu_custom_call" | custom-call | tf_op jit(solution)/shard_map/pallas_call | solution.py:68
  27.4 7.7 %shard_map.164 = (bf16[128,512]{1,0:T(8,128)(2,1)}, bf16[128,256]{1,0:T(8,128)(2,1)}) custom-call(s32[1]{0:T(128)} %bitcast.start_ref, bf16[1024,640]{1,0:T(8,128)(2,1)} %shard_map.163.joined_ref, bf16[8,128,128]{2,1,0:T(8,128)(2,1)} %maximum_maximum_fusion.nope_ref, bf16[8,128,128]{2,1,0:T(8,128)(2,1)} %fusion.11.rope_ref, bf16[512,512]{1,0:T(8,128)(2,1)} %key_major_ref.1, ...), custom_call_target="tpu_custom_call" | custom-call | tf_op jit(solution)/shard_map/pallas_call | solution.py:919
  35.1 0.0 copy-start.3
  35.1 0.0 copy-done.1
  35.1 1.2 %fusion.16 = f32[128,2048]{1,0:T(8,128)S(1)} fusion(bf16[128,256]{1,0:T(8,128)(2,1)} %get-tuple-element.8, bf16[256,2048]{1,0:T(8,128)(2,1)S(1)} %copy-done.1), kind=kOutput, calls=%fused_computation.41 | convolution fusion | flops 134217728 | bytes 2162688 | tf_op jit(solution)/shard_map/dot_general | solution.py:945
  36.3 0.0 copy-done
  36.3 0.0 copy-done.3
  36.3 1.3 %fusion.part_ref = bf16[128,2048]{1,0:T(8,128)(2,1)} fusion(f32[128,2048]{1,0:T(8,128)S(1)} %fusion.16, bf16[128,512]{1,0:T(8,128)(2,1)S(1)} %copy-done.3, bf16[512,2048]{1,0:T(8,128)(2,1)S(1)} %copy-done), kind=kOutput, calls=%fused_computation.1 | convolution fusion | flops 268959744 | bytes 3801088 | tf_op jit(solution)/shard_map/dot_general | solution.py:944
  37.6 11.1 %shard_map.165.x_ref = bf16[128,512]{1,0:T(8,128)(2,1)} custom-call(bf16[128,2048]{1,0:T(8,128)(2,1)} %fusion.part_ref, bf16[128,512]{1,0:T(8,128)(2,1)} %res_ref.1), custom_call_target="tpu_custom_call" | custom-call | tf_op jit(solution)/shard_map/pallas_call | solution.py:68
  48.6 49.3 %shard_map.166 = bf16[128,512]{1,0:T(8,128)(2,1)} custom-call(bf16[128,512]{1,0:T(8,128)(2,1)} %shard_map.165.x_ref, s32[128,2]{1,0:T(8,128)} %copy.47.ids_ref, s32[2,128]{1,0:T(2,128)} %bitcast.24, f32[128,2]{1,0:T(8,128)} %copy.48.mix_ref, f32[1,2048]{1,0:T(1,128)} %bitcast.23, bf16[1,2048,1024]{2,1,0:T(8,128)(2,1)} %gate_ref.1, ...), custom_call_target="tpu_custom_call" | custom-call | tf_op jit(solution)/shard_map/pallas_call | solution.py:789
  97.9 1.6 %copy.55 = bf16[128,512]{1,0:T(8,128)(2,1)} copy(bf16[128,512]{1,0:T(8,128)(2,1)} %shard_map.166) | data formatting | bytes 262144
  (8 shorter events, 0.1 us)
Async XLA Ops:
  0.0 36.3 %copy-start = (bf16[512,2048]{1,0:T(8,128)(2,1)S(1)}, bf16[512,2048]{1,0:T(8,128)(2,1)}, u32[]{:S(2)}) copy-start(bf16[512,2048]{1,0:T(8,128)(2,1)} %param.25) | copy-start | bytes 6291460
  0.0 7.6 %copy-start.2 = (bf16[128,768]{1,0:T(8,128)(2,1)S(1)}, bf16[128,768]{1,0:T(8,128)(2,1)}, u32[]{:S(2)}) copy-start(bf16[128,768]{1,0:T(8,128)(2,1)} %param.17) | copy-start | bytes 589828
  10.1 25.0 %copy-start.1 = (bf16[256,2048]{1,0:T(8,128)(2,1)S(1)}, bf16[256,2048]{1,0:T(8,128)(2,1)}, u32[]{:S(2)}) copy-start(bf16[256,2048]{1,0:T(8,128)(2,1)} %param.26) | copy-start | bytes 3145732
  35.1 1.2 %copy-start.3 = (bf16[128,512]{1,0:T(8,128)(2,1)S(1)}, bf16[128,512]{1,0:T(8,128)(2,1)}, u32[]{:S(2)}) copy-start(bf16[128,512]{1,0:T(8,128)(2,1)} %get-tuple-element.7) | copy-start | bytes 393220

commit v2 on v1

--- a/solution.py
+++ b/solution.py
@@ -2,6 +2,7 @@
 
 import jax
 import jax.numpy as jnp
+import numpy as np
 from jax import lax
 from jax.experimental import pallas as pl
 from jax.experimental.pallas import tpu as pltpu
@@ -821,6 +822,387 @@
     )(stream_mid, ids, ids.T, mix, gain.reshape(1, -1), gate_proj, up_proj, down_proj)
 
 
+def rope_table(count, width):
+    half_width = width // 2
+    inverse_freq = (1.0 / theta_base ** (np.arange(half_width, dtype=np.float32) * (2.0 / width))).astype(np.float32)
+    angles = np.arange(count, dtype=np.float32)[:, None] * inverse_freq[None, :]
+    cosine, sine = np.cos(angles), np.sin(angles)
+    return np.concatenate([cosine, cosine, -sine, sine], axis=1).astype(np.float32)
+
+
+def attend_kernel(
+    sp,
+    heads,
+    q_major_ref,
+    q_minor_ref,
+    latent_ref,
+    rope_ref,
+    table_ref,
+    key_major_ref,
+    value_major_ref,
+    key_minor_ref,
+    value_minor_ref,
+    out_major_ref,
+    out_minor_ref,
+    res_ref,
+    stream_ref,
+    q_major,
+    q_minor,
+    rope_raw,
+    table,
+    weights,
+    projection,
+    residual,
+    blocks,
+    queries,
+    kept,
+    tops,
+    sums,
+    gathered_out,
+    mixed,
+    part,
+    landed,
+    turned,
+    load_sem,
+    z_send,
+    z_recv,
+    t_send,
+    t_recv,
+    s_send,
+    s_recv,
+    r_send,
+    r_recv,
+):
+    heads_major, heads_minor = heads
+    tok_rows, latent = latent_ref.shape
+    rope_width = rope_ref.shape[1]
+    chips = sp // 2
+    tp = 4
+    quarter = tok_rows // tp
+    pack = 128 // NOPE_MINOR
+    sp_id, tp_id = lax.axis_index("sp"), lax.axis_index("tp")
+    level, core = sp_id // 2, lax.rem(sp_id, 2)
+    sibling = flip(sp_id, 1)
+    near, far, across = square(tp_id)
+    f32, bf16 = jnp.float32, jnp.bfloat16
+
+    loads = []
+
+    def load(src, dst):
+        copy = pltpu.make_async_copy(src, dst, load_sem.at[len(loads)])
+        copy.start()
+        loads.append(copy)
+        return copy
+
+    own_rows = pl.ds(pl.multiple_of(sp_id * tok_rows, tok_rows), tok_rows)
+    early = [
+        load(latent_ref, blocks.at[0, 0, :, pl.ds(0, latent)]),
+        load(rope_ref, rope_raw),
+        load(table_ref.at[own_rows, :], table),
+    ]
+    asked = [load(q_major_ref, q_major), load(q_minor_ref, q_minor)]
+    spans, first = [], 0
+    for ref in (key_major_ref, key_minor_ref, value_major_ref, value_minor_ref):
+        span = pl.ds(first, ref.shape[1])
+        asked.append(load(ref, weights.at[:, span]))
+        spans.append(span)
+        first += ref.shape[1]
+    split = out_major_ref.shape[0]
+    late = [
+        load(out_major_ref, projection.at[pl.ds(0, split), :]),
+        load(out_minor_ref, projection.at[pl.ds(split, out_minor_ref.shape[0]), :]),
+        load(res_ref, residual),
+    ]
+
+    barrier = pltpu.get_barrier_semaphore()
+    for offset in range(1, chips):
+        pl.semaphore_signal(barrier, inc=1, device_id=(flip(sp_id, 2 * offset), tp_id), device_id_type=MESH)
+    pl.semaphore_signal(barrier, inc=1, device_id=(sibling, tp_id), device_id_type=MESH)
+    for peer in (near, far, across):
+        pl.semaphore_signal(barrier, inc=1, device_id=(sp_id, peer), device_id_type=MESH)
+
+    half = rope_width // 2
+
+    def rotate(x):
+        x = x.astype(f32)
+        swapped = jnp.concatenate([x[:, half:], x[:, :half]], axis=1)
+        return (x * table[:, :rope_width] + swapped * table[:, rope_width:]).astype(bf16)
+
+    for copy in early:
+        copy.wait()
+    tail = blocks.shape[3] - latent
+    pad = jnp.zeros((tok_rows, tail - rope_width), bf16)
+    blocks[0, 0, :, latent:] = jnp.concatenate([rotate(rope_raw[...]), pad], axis=1)
+    pl.semaphore_wait(barrier, chips - 1 + 1 + 3)
+
+    own_quarter = pl.ds(pl.multiple_of(tp_id * quarter, quarter), quarter)
+
+    def lift(d):
+        return remote(
+            blocks.at[0, 0, own_quarter, :],
+            blocks.at[d, 0, own_quarter, :],
+            z_send.at[d],
+            z_recv.at[d],
+            sp_id + 2 * d,
+            tp_id,
+        )
+
+    def spread(d, slot):
+        place = blocks.at[d, 0, own_quarter, :]
+        return remote(place, place, t_send.at[d, slot], t_recv.at[d, slot], sp_id, (near, far, across)[slot])
+
+    def share(d):
+        return remote(blocks.at[d, 0], blocks.at[d, 1], s_send.at[d], s_recv.at[d], sibling, tp_id)
+
+    for d in range(1, chips):
+
+        @pl.when(level + d < chips)
+        def _():
+            lift(d).start()
+
+    share(0).start()
+
+    for copy in asked:
+        copy.wait()
+    zeros = jnp.zeros((tok_rows, 128 - rope_width), bf16)
+    lanes = lax.broadcasted_iota(jnp.int32, (tok_rows, 128), 1)
+    for h in range(heads_major):
+        first = h * (NOPE_MAJOR + rope_width)
+        queries[h, :, :128] = q_major[:, first : first + NOPE_MAJOR]
+        turned_part = rotate(q_major[:, first + NOPE_MAJOR : first + NOPE_MAJOR + rope_width])
+        queries[h, :, 128:] = jnp.concatenate([turned_part, zeros], axis=1)
+    blank = jnp.zeros((tok_rows, NOPE_MINOR), bf16)
+    for h in range(heads_minor):
+        first = h * (NOPE_MINOR + rope_width)
+        member = h % pack
+        nope = q_minor[:, first : first + NOPE_MINOR]
+        row = [blank] * member + [nope] + [blank] * (pack - 1 - member)
+        queries[heads_major + h, :, :128] = jnp.concatenate(row, axis=1)
+        turned_part = rotate(q_minor[:, first + NOPE_MINOR : first + NOPE_MINOR + rope_width])
+        queries[heads_major + h, :, 128:] = jnp.concatenate([turned_part, zeros], axis=1)
+
+    keys = 2 * tok_rows
+    log2e = 1.4426950408889634
+    contract = (((1,), (1,)), ((), ()))
+
+    def project(d):
+        for q in range(2):
+            rows = blocks[d, q, :, :latent]
+            kept[pl.ds(q * tok_rows, tok_rows), :] = jnp.dot(rows, weights[...], preferred_element_type=f32).astype(
+                bf16
+            )
+
+    def attend(d):
+        tails = jnp.concatenate([blocks[d, 0, :, latent:], blocks[d, 1, :, latent:]], axis=0)
+        for h in range(heads_major + heads_minor):
+            if h < heads_major:
+                tile, scale = h, (NOPE_MAJOR + rope_width) ** (-0.5)
+                key_at, value_at = tile * 128, spans[2].start + tile * 128
+            else:
+                tile, scale = (h - heads_major) // pack, (NOPE_MINOR + rope_width) ** (-0.5)
+                key_at, value_at = spans[1].start + tile * 128, spans[3].start + tile * 128
+            key = jnp.concatenate([kept[:, key_at : key_at + 128], tails], axis=1)
+            scores = lax.dot_general(queries[h], key, contract, preferred_element_type=f32) * (scale * log2e)
+            if d == 0:
+                spot = lax.broadcasted_iota(jnp.int32, (tok_rows, keys), 1)
+                row = lax.broadcasted_iota(jnp.int32, (tok_rows, keys), 0)
+                limit = jnp.where(spot < tok_rows, row, keys * core - 1)
+                scores = jnp.where(spot <= limit, scores, -jnp.inf)
+            peak = jnp.max(scores, axis=1, keepdims=True)
+            if d > 0:
+                before = tops[h][:, :1]
+                peak = jnp.maximum(before, peak)
+                fade = jnp.exp2(before - peak)
+            chance = jnp.exp2(scores - peak)
+            total = jnp.sum(chance, axis=1, keepdims=True)
+            summed = jnp.dot(chance.astype(bf16), kept[:, value_at : value_at + 128], preferred_element_type=f32)
+            if d > 0:
+                total = total + sums[h][:, :1] * fade
+                summed = summed + gathered_out[h] * fade
+            tops[h] = jnp.broadcast_to(peak, (tok_rows, 128))
+            sums[h] = jnp.broadcast_to(total, (tok_rows, 128))
+            gathered_out[h] = summed
+
+    def arrival(place, sem):
+        return pltpu.make_async_copy(place, place, sem)
+
+    share(0).wait_recv()
+    project(0)
+
+    for d in range(1, chips):
+        if d == 2 or chips == 2:
+            attend(0)
+
+        @pl.when(level >= d)
+        def _():
+            arrival(blocks.at[d, 0, own_quarter, :], z_recv.at[d]).wait()
+            for slot in range(3):
+                spread(d, slot).start()
+
+    for d in range(1, chips):
+
+        @pl.when(level >= d)
+        def _():
+            for slot in range(3):
+                spread(d, slot).wait_recv()
+            share(d).start()
+
+    for d in range(1, chips):
+
+        @pl.when(level >= d)
+        def _():
+            share(d).wait_recv()
+            project(d)
+            attend(d)
+
+    for h in range(heads_major):
+        mixed[:, h * 128 : h * 128 + 128] = (gathered_out[h] / sums[h]).astype(bf16)
+    for tile in range(-(-heads_minor // pack)):
+        result = None
+        for member in range(min(pack, heads_minor - tile * pack)):
+            h = heads_major + tile * pack + member
+            value = gathered_out[h] / sums[h]
+            result = value if result is None else jnp.where(lanes < member * NOPE_MINOR, result, value)
+        first = (heads_major + tile) * 128
+        mixed[:, first : first + 128] = result.astype(bf16)
+
+    width = stream_ref.shape[1]
+    for copy in late:
+        copy.wait()
+
+    def columns(owner):
+        return pl.ds(pl.multiple_of(owner * width, width), width)
+
+    mid = tok_rows // 2
+    halves = (pl.ds(0, mid), pl.ds(mid, mid))
+    rows = mixed[...]
+    started = []
+
+    def fill(owner):
+        part[:, columns(owner)] = jnp.dot(rows, projection[:, columns(owner)], preferred_element_type=f32).astype(bf16)
+
+    def push(src, slot, target):
+        copy = remote(src, landed.at[slot], r_send.at[slot], r_recv.at[slot], sp_id, target)
+        copy.start()
+        started.append(copy)
+        return copy
+
+    fill(across)
+    second = push(part.at[halves[0], columns(across)], 1, near)
+    fourth = push(part.at[halves[1], columns(across)], 3, far)
+    fill(near)
+    first = push(part.at[halves[0], columns(near)], 0, near)
+    fill(far)
+    third = push(part.at[halves[1], columns(far)], 2, far)
+    fill(tp_id)
+    second.wait_recv()
+    turned[0] = (part[halves[0], columns(far)].astype(f32) + landed[1].astype(f32)).astype(bf16)
+    fifth = push(turned.at[0], 4, far)
+    fourth.wait_recv()
+    turned[1] = (part[halves[1], columns(near)].astype(f32) + landed[3].astype(f32)).astype(bf16)
+    sixth = push(turned.at[1], 5, near)
+    for q, plain, summed in ((0, first, fifth), (1, third, sixth)):
+        plain.wait_recv()
+        value = part[halves[q], columns(tp_id)].astype(f32) + residual[halves[q], :].astype(f32)
+        value = value + landed[2 * q].astype(f32)
+        summed.wait_recv()
+        stream_ref[halves[q], :] = (value + landed[4 + q].astype(f32)).astype(bf16)
+
+    for copy in started:
+        copy.wait_send()
+    share(0).wait_send()
+    for d in range(1, chips):
+
+        @pl.when(level + d < chips)
+        def _():
+            lift(d).wait_send()
+
+        @pl.when(level >= d)
+        def _():
+            share(d).wait_send()
+            for slot in range(3):
+                spread(d, slot).wait_send()
+
+
+def fused_attention(
+    sp,
+    query_major,
+    query_minor,
+    latent_rows,
+    rope_keys,
+    key_up_major,
+    value_up_major,
+    key_up_minor,
+    value_up_minor,
+    out_major,
+    out_minor,
+    residual,
+):
+    tok_rows, latent = latent_rows.shape
+    rope_width = rope_keys.shape[1]
+    width = residual.shape[1]
+    chips = sp // 2
+    heads = (key_up_major.shape[1] // NOPE_MAJOR, key_up_minor.shape[1] // NOPE_MINOR)
+    count = heads[0] + heads[1]
+    joined = latent + rope_width + -(latent + rope_width) % 128
+    kept = key_up_major.shape[1] + key_up_minor.shape[1] + value_up_major.shape[1] + value_up_minor.shape[1]
+    mixed = value_up_major.shape[1] + value_up_minor.shape[1]
+    dma = pltpu.SemaphoreType.DMA
+    bf16 = jnp.bfloat16
+    table = jnp.asarray(rope_table(sp * tok_rows, rope_width))
+    operands = (
+        query_major,
+        query_minor,
+        latent_rows,
+        rope_keys,
+        table,
+        key_up_major,
+        value_up_major,
+        key_up_minor,
+        value_up_minor,
+        out_major,
+        out_minor,
+        residual,
+    )
+    return pl.pallas_call(
+        functools.partial(attend_kernel, sp, heads),
+        out_shape=jax.ShapeDtypeStruct((tok_rows, width), bf16),
+        in_specs=[pl.BlockSpec(memory_space=pl.ANY)] * len(operands),
+        out_specs=pl.BlockSpec(memory_space=pltpu.VMEM),
+        scratch_shapes=[
+            pltpu.VMEM(query_major.shape, bf16),
+            pltpu.VMEM(query_minor.shape, bf16),
+            pltpu.VMEM(rope_keys.shape, bf16),
+            pltpu.VMEM((tok_rows, 2 * rope_width), jnp.float32),
+            pltpu.VMEM((latent, kept), bf16),
+            pltpu.VMEM((mixed, out_major.shape[1]), bf16),
+            pltpu.VMEM(residual.shape, bf16),
+            pltpu.VMEM((chips, 2, tok_rows, joined), bf16),
+            pltpu.VMEM((count, tok_rows, 256), bf16),
+            pltpu.VMEM((2 * tok_rows, kept), bf16),
+            pltpu.VMEM((count, tok_rows, 128), jnp.float32),
+            pltpu.VMEM((count, tok_rows, 128), jnp.float32),
+            pltpu.VMEM((count, tok_rows, 128), jnp.float32),
+            pltpu.VMEM((tok_rows, mixed), bf16),
+            pltpu.VMEM((tok_rows, out_major.shape[1]), bf16),
+            pltpu.VMEM((6, tok_rows // 2, width), bf16),
+            pltpu.VMEM((2, tok_rows // 2, width), bf16),
+            dma((len(operands),)),
+            dma((chips,)),
+            dma((chips,)),
+            dma((chips, 3)),
+            dma((chips, 3)),
+            dma((chips,)),
+            dma((chips,)),
+            dma((6,)),
+            dma((6,)),
+        ],
+        compiler_params=pltpu.CompilerParams(
+            collective_id=5, has_side_effects=True, vmem_limit_bytes=60 * 1024 * 1024
+        ),
+    )(*operands)
+
+
 def run_experts(rows, gain, gate_proj, up_proj, down_proj):
     slots, features = rows.shape
     units = gate_proj.shape[2]
@@ -871,6 +1253,27 @@
     down_proj,
 ):
     tok_rows = query_major.shape[0]
+    fast = tp == 4 and sp & (sp - 1) == 0
+    fast = fast and tok_rows % 64 == 0 and (2 * tok_rows * TOP // sp) % 16 == 0
+    fast = fast and key_up_major.shape[1] % 128 == 0 and key_up_minor.shape[1] % 128 == 0
+    if fast:
+        stream_mid = fused_attention(
+            sp,
+            query_major,
+            query_minor,
+            latent_rows,
+            rope_keys,
+            key_up_major,
+            value_up_major,
+            key_up_minor,
+            value_up_minor,
+            out_major,
+            out_minor,
+            residual,
+        )
+        return fused_experts(
+            sp, tp, stream_mid, expert_ids, expert_weights, norm_gain, gate_proj, up_proj, down_proj
+        )
     row_start = lax.axis_index("sp") * tok_rows
     positions = row_start + jnp.arange(tok_rows, dtype=jnp.int32)
     rope_width = rope_keys.shape[1]
@@ -953,10 +1356,6 @@
         1,
         (partial_value.astype(jnp.bfloat16), residual),
     )
-    if tp == 4 and sp & (sp - 1) == 0 and (2 * tok_rows * TOP // sp) % 16 == 0:
-        return fused_experts(
-            sp, tp, stream_mid, expert_ids, expert_weights, norm_gain, gate_proj, up_proj, down_proj
-        )
     experts = sp
     capacity = 2 * tok_rows * TOP // experts
     slots = experts * capacity

time: 101 us -> 89.4 us (0.89)
  other arithmetic: 4.88 us -> 0 us
  Pallas kernels: 85.3 us -> 82.3 us
  matrix products: 2.44 us -> 0 us
    pallas_call x3 -> x1, Pallas kernels: 36 us -> 30.2 us  [fused_attention(): pl.pallas_call(functools.partial(attend_kernel, sp, heads), out_shape=jax...]
    concatenate x3 -> x0, other arithmetic: 3.26 us -> none  [the longest x1 1.67 us: per_device(): jnp.concatenate([latent_rows, rope_rot, jnp.zeros((tok_rows, -(latent + r...]
    pallas_call x1, Pallas kernels: 49.3 us -> 52.1 us  [fused_experts(): pl.pallas_call(functools.partial(moe_kernel, sp), out_shape=jax.ShapeDtyp...]
    dot_general x2 -> x0, matrix products: 2.44 us -> none  [the longest x1 1.26 us: per_device(): jnp.dot(attn_major, out_major, preferred_element_type=jnp.float32)]
    unnamed x18 -> x4, local copies, waits for them, and re-layouts: 6.23 us -> 5.8 us
where the time goes in v2:
time: 89.4 us; the launch traced here: 88.1 us
  Pallas kernels  82.3 us (92%)
  local copies, waits for them, and re-layouts  5.8 us (6%)
    pallas_call x1, Pallas kernels, fused_experts(): pl.pallas_call(functools.partial(moe_kernel, sp), out_shape=jax.ShapeDtyp...  52.1 us
    pallas_call x1, Pallas kernels, fused_attention(): pl.pallas_call(functools.partial(attend_kernel, sp, heads), out_shape=jax...  30.2 us
    unnamed x4, local copies, waits for them, and re-layouts  5.8 us

profile of v2, /device:TPU:25, one launch (start us, length us, event | category | flops | bytes accessed | tf_op | source)
XLA Modules:
  0.0 88.1 jit_solution(1572127820919236067)
XLA Ops:
  0.0 1.4 %copy.19.rope_ref = bf16[128,64]{1,0:T(8,128)(2,1)} copy(bf16[128,64]{0,1:T(8,128)(2,1)} %param.21) | data formatting | bytes 32768 | tf_op args[3]
  1.4 1.4 %copy.21.mix_ref = f32[128,2]{1,0:T(8,128)} copy(f32[128,2]{0,1:T(2,128)} %param.31) | data formatting | bytes 2048 | tf_op args[13]
  2.8 1.4 %copy.20.ids_ref = s32[128,2]{1,0:T(8,128)} copy(s32[128,2]{0,1:T(2,128)} %param.30) | data formatting | bytes 2048 | tf_op args[12]
  4.2 30.2 %shard_map.172.x_ref = bf16[128,512]{1,0:T(8,128)(2,1)} custom-call(bf16[128,768]{1,0:T(8,128)(2,1)} %q_major_ref.1, bf16[128,512]{1,0:T(8,128)(2,1)} %q_minor_ref.1, bf16[128,512]{1,0:T(8,128)(2,1)} %latent_ref.1, bf16[128,64]{1,0:T(8,128)(2,1)} %copy.19.rope_ref, f32[1024,128]{1,0:T(8,128)} %constant.2.clone.table_ref, bf16[512,512]{1,0:T(8,128)(2,1)} %key_major_ref.1, ...), custom_call_target="tpu_custom_call" | custom-call | tf_op jit(solution)/shard_map/pallas_call | solution.py:1167
  34.4 52.1 %shard_map.173 = bf16[128,512]{1,0:T(8,128)(2,1)} custom-call(bf16[128,512]{1,0:T(8,128)(2,1)} %shard_map.172.x_ref, s32[128,2]{1,0:T(8,128)} %copy.20.ids_ref, s32[2,128]{1,0:T(2,128)} %bitcast.3, f32[128,2]{1,0:T(8,128)} %copy.21.mix_ref, f32[1,2048]{1,0:T(1,128)} %bitcast.2, bf16[1,2048,1024]{2,1,0:T(8,128)(2,1)} %gate_ref.1, ...), custom_call_target="tpu_custom_call" | custom-call | tf_op jit(solution)/shard_map/pallas_call | solution.py:790
  86.5 1.6 %copy.23 = bf16[128,512]{1,0:T(8,128)(2,1)} copy(bf16[128,512]{1,0:T(8,128)(2,1)} %shard_map.173) | data formatting | bytes 262144

commit v3 on v0

--- a/solution.py
+++ b/solution.py
@@ -2,6 +2,7 @@
 
 import jax
 import jax.numpy as jnp
+import numpy as np
 from jax import lax
 from jax.experimental import pallas as pl
 from jax.experimental.pallas import tpu as pltpu
@@ -501,6 +502,780 @@
         out_ref[...] = part.astype(jnp.bfloat16)
 
 
+def flip(index, offset):
+    step = 1
+    while step <= offset:
+        if offset & step:
+            index = index + step * (1 - 2 * lax.rem(index // step, 2))
+        step *= 2
+    return index
+
+
+def rope_table(count, width):
+    half_width = width // 2
+    inverse_freq = (1.0 / theta_base ** (np.arange(half_width, dtype=np.float32) * (2.0 / width))).astype(np.float32)
+    angles = np.arange(count, dtype=np.float32)[:, None] * inverse_freq[None, :]
+    cosine, sine = np.cos(angles), np.sin(angles)
+    return np.concatenate([cosine, cosine, -sine, sine], axis=1).astype(np.float32)
+
+
+def plans(chips):
+    last = chips - 1
+    simple = {"streamed": [("open", 0), ("relay", 0)]}
+    for k in range(last):
+        simple[f"between {k}"] = [("open", k + 1)]
+        simple[f"after {k}"] = [("relay", k + 1)] + ([("turn", k - 1)] if k else [])
+    simple[f"after {last}"] = [("turn", last - 1)] if last else []
+    simple[f"after {last}"] += [("turn", last)] + [("close", k) for k in range(chips)]
+    if chips != 4:
+        return [simple] * chips
+    low = {
+        "streamed": [("open", 0), ("relay", 0)],
+        "between 0": [("open", 1)],
+        "after 0": [("relay", 1), ("open", 2)],
+        "between 1": [("relay", 2)],
+        "after 1": [("turn", 0)],
+        "between 2": [("open", 3)],
+        "after 2": [("relay", 3), ("turn", 1), ("close", 0), ("turn", 2), ("close", 1)],
+        "after 3": [("close", 2), ("turn", 3), ("close", 3)],
+    }
+    early = {
+        "pushed": [("open", 0)],
+    }
+    ending = {
+        "after 2": [("turn", 1), ("close", 0)],
+        "after 3": [("turn", 2), ("close", 1), ("turn", 3), ("close", 2), ("close", 3)],
+    }
+    upper = {
+        "streamed": [("relay", 0), ("open", 1), ("open", 2), ("relay", 1)],
+        "between 0": [("relay", 2)],
+        "between 1": [("open", 3)],
+        "after 1": [("relay", 3), ("turn", 0)],
+    }
+    top = {
+        "streamed": [("relay", 0), ("open", 3), ("open", 1), ("relay", 1), ("open", 2)],
+        "between 0": [("relay", 2)],
+        "after 0": [("relay", 3)],
+        "after 1": [("turn", 0)],
+    }
+    return [low, low, early | upper | ending, early | top | ending]
+
+
+def layer_kernel(
+    sp,
+    heads,
+    q_major_ref,
+    q_minor_ref,
+    latent_ref,
+    rope_ref,
+    table_ref,
+    key_major_ref,
+    value_major_ref,
+    key_minor_ref,
+    value_minor_ref,
+    out_major_ref,
+    out_minor_ref,
+    res_ref,
+    ids_ref,
+    mix_ref,
+    gain_ref,
+    gate_ref,
+    up_ref,
+    down_ref,
+    out_ref,
+    q_major,
+    q_minor,
+    rope_raw,
+    table,
+    weights,
+    projection,
+    residual,
+    ids,
+    mix,
+    gain,
+    gate,
+    up,
+    down,
+    blocks,
+    queries,
+    kept,
+    tops,
+    scores,
+    chances,
+    fades,
+    gathered_out,
+    mixed,
+    spread_part,
+    spread_landed,
+    spread_turned,
+    stream,
+    select,
+    hot,
+    mix_column,
+    placed,
+    rows_in,
+    normed,
+    hidden,
+    part,
+    landed,
+    turned,
+    summed,
+    returned,
+    load_sem,
+    expert_sem,
+    l_send,
+    l_recv,
+    q_send,
+    q_recv,
+    s_send,
+    s_recv,
+    o_send,
+    o_recv,
+    z_send,
+    z_recv,
+    t_send,
+    t_recv,
+    r_send,
+    r_recv,
+    y_send,
+    y_recv,
+):
+    heads_major, heads_minor = heads
+    tok_rows, latent = latent_ref.shape
+    rope_width = rope_ref.shape[0]
+    chips = sp // 2
+    tp = 4
+    quarter = tok_rows // tp
+    pack = 128 // NOPE_MINOR
+    sp_id, tp_id = lax.axis_index("sp"), lax.axis_index("tp")
+    level, core = sp_id // 2, lax.rem(sp_id, 2)
+    sibling = flip(sp_id, 1)
+    near, far, across = square(tp_id)
+    f32, bf16 = jnp.float32, jnp.bfloat16
+
+    loads = []
+
+    def load(src, dst):
+        copy = pltpu.make_async_copy(src, dst, load_sem.at[len(loads)])
+        copy.start()
+        loads.append(copy)
+        return copy
+
+    own_rows = pl.ds(pl.multiple_of(sp_id * tok_rows, tok_rows), tok_rows)
+    early = [
+        load(latent_ref, blocks.at[0, 0, :, pl.ds(0, latent)]),
+        load(rope_ref, rope_raw),
+        load(table_ref.at[own_rows, :], table),
+    ]
+    asked = [load(q_major_ref, q_major), load(q_minor_ref, q_minor)]
+    spans, first = [], 0
+    for ref in (key_major_ref, key_minor_ref, value_major_ref, value_minor_ref):
+        span = pl.ds(first, ref.shape[1])
+        asked.append(load(ref, weights.at[:, span]))
+        spans.append(span)
+        first += ref.shape[1]
+    split = out_major_ref.shape[0]
+    routing = [load(ids_ref, ids), load(mix_ref, mix), load(gain_ref, gain)]
+    late = [
+        load(out_major_ref, projection.at[pl.ds(0, split), :]),
+        load(out_minor_ref, projection.at[pl.ds(split, out_minor_ref.shape[0]), :]),
+        load(res_ref, residual),
+    ]
+
+    barrier = pltpu.get_barrier_semaphore()
+    for offset in range(1, sp):
+        pl.semaphore_signal(barrier, inc=1, device_id=(flip(sp_id, offset), tp_id), device_id_type=MESH)
+    for peer in (near, far, across):
+        pl.semaphore_signal(barrier, inc=1, device_id=(sp_id, peer), device_id_type=MESH)
+
+    lane = lax.broadcasted_iota(jnp.int32, (tok_rows, 128), 1)
+    low = lane < rope_width
+
+    def rotator(cosine, back, ahead):
+        def rotate(x):
+            return x * cosine + pltpu.roll(x, 128 - rope_width // 2, 1) * back + pltpu.roll(x, rope_width // 2, 1) * ahead
+
+        return rotate
+
+    for copy in early:
+        copy.wait()
+    trig = table[...]
+    flipped = pltpu.roll(trig, 64, 1)
+    half = rope_width // 2
+    rotate_low = rotator(
+        jnp.where(low, trig, 1.0),
+        jnp.where(lane < half, flipped, 0.0),
+        jnp.where((lane >= half) & low, flipped, 0.0),
+    )
+    rotate_high = rotator(
+        jnp.where(low, 1.0, flipped),
+        jnp.where(low | (lane >= 64 + half), 0.0, trig),
+        jnp.where(lane >= 64 + half, trig, 0.0),
+    )
+    raw = rope_raw[...].astype(f32)
+    raw = jnp.concatenate([raw, jnp.zeros((128 - rope_width, tok_rows), f32)], axis=0).T
+    blocks[0, 0, :, latent:] = rotate_low(raw).astype(bf16)
+    pl.semaphore_wait(barrier, sp - 1 + 3)
+
+    own_quarter = pl.ds(pl.multiple_of(tp_id * quarter, quarter), quarter)
+
+    def lift(d):
+        return remote(
+            blocks.at[0, 0, own_quarter, :],
+            blocks.at[d, 0, own_quarter, :],
+            l_send.at[d],
+            l_recv.at[d],
+            sp_id + 2 * d,
+            tp_id,
+        )
+
+    def spread(d, slot):
+        place = blocks.at[d, 0, own_quarter, :]
+        return remote(place, place, q_send.at[d, slot], q_recv.at[d, slot], sp_id, (near, far, across)[slot])
+
+    def share(d):
+        return remote(blocks.at[d, 0], blocks.at[d, 1], s_send.at[d], s_recv.at[d], sibling, tp_id)
+
+    for d in range(1, chips):
+
+        @pl.when(level + d < chips)
+        def _():
+            lift(d).start()
+
+    share(0).start()
+
+    for copy in asked:
+        copy.wait()
+    expert_loads = []
+    pieces = expert_sem.shape[1]
+    for index, (src, dst) in enumerate(((gate_ref, gate), (up_ref, up), (down_ref, down))):
+        count = dst.shape[0] // pieces
+        for piece in range(pieces):
+            span = pl.ds(piece * count, count)
+            copy = pltpu.make_async_copy(src.at[0, span, :], dst.at[span, :], expert_sem.at[index, piece])
+            copy.start()
+            expert_loads.append(copy)
+    def column(ref, index):
+        return ref[:, index * 128 : index * 128 + 128].astype(f32)
+
+    def only_low(x):
+        return jnp.where(low, x, 0.0).astype(bf16)
+
+    for pair in range(heads_major // 2):
+        one, two = column(q_major, 3 * pair + 1), column(q_major, 3 * pair + 2)
+        queries[2 * pair, :, :128] = q_major[:, pair * 384 : pair * 384 + 128]
+        queries[2 * pair, :, 128:] = only_low(rotate_low(one))
+        queries[2 * pair + 1, :, :128] = jnp.where(low, pltpu.roll(one, 64, 1), pltpu.roll(two, 64, 1)).astype(bf16)
+        queries[2 * pair + 1, :, 128:] = only_low(pltpu.roll(rotate_high(two), 64, 1))
+    for h in range(heads_minor):
+        whole = rotate_high(column(q_minor, h))
+        moved = pltpu.roll(whole, 64, 1)
+        queries[heads_major + h, :, 128:] = only_low(moved)
+        if h % pack == 0:
+            queries[heads_major + h, :, :128] = only_low(whole)
+        else:
+            queries[heads_major + h, :, :128] = jnp.where(low, 0.0, moved).astype(bf16)
+
+    keys = 2 * tok_rows
+    log2e = 1.4426950408889634
+    contract = (((1,), (1,)), ((), ()))
+
+    def project(d):
+        for q in range(2):
+            rows = blocks[d, q, :, :latent]
+            kept[pl.ds(q * tok_rows, tok_rows), :] = jnp.dot(rows, weights[...], preferred_element_type=f32).astype(
+                bf16
+            )
+
+    everyone = range(heads_major + heads_minor)
+
+    def tile_of(h):
+        return h if h < heads_major else (h - heads_major) // pack
+
+    def attend(d):
+        tails = jnp.concatenate([blocks[d, 0, :, latent:], blocks[d, 1, :, latent:]], axis=0)
+        for h in everyone:
+            nope = NOPE_MAJOR if h < heads_major else NOPE_MINOR
+            key_at = tile_of(h) * 128 + (0 if h < heads_major else spans[1].start)
+            key = jnp.concatenate([kept[:, key_at : key_at + 128], tails], axis=1)
+            scale = (nope + rope_width) ** (-0.5) * log2e
+            value = lax.dot_general(queries[h], key, contract, preferred_element_type=f32) * scale
+            if d == 0:
+                spot = lax.broadcasted_iota(jnp.int32, (tok_rows, keys), 1)
+                row = lax.broadcasted_iota(jnp.int32, (tok_rows, keys), 0)
+                limit = jnp.where(spot < tok_rows, row, keys * core - 1)
+                value = jnp.where(spot <= limit, value, -jnp.inf)
+            scores[h] = value
+        for h in everyone:
+            value = scores[h]
+            peak = jnp.max(value, axis=1, keepdims=True)
+            if d > 0:
+                before = tops[h][:, :1]
+                peak = jnp.maximum(before, peak)
+                fades[h] = jnp.broadcast_to(jnp.exp2(before - peak), (tok_rows, 128))
+            chances[h] = jnp.exp2(value - peak).astype(bf16)
+            tops[h] = jnp.broadcast_to(peak, (tok_rows, 128))
+        ones = jnp.ones((keys, 128), bf16)
+        for h in everyone:
+            value_at = tile_of(h) * 128 + (spans[2].start if h < heads_major else spans[3].start)
+            value = jnp.concatenate([kept[:, value_at : value_at + 128], ones], axis=1)
+            summed = jnp.dot(chances[h], value, preferred_element_type=f32)
+            if d == 0:
+                gathered_out[h] = summed
+            else:
+                fade = fades[h]
+                gathered_out[h, :, :128] = summed[:, :128] + gathered_out[h, :, :128] * fade
+                gathered_out[h, :, 128:] = summed[:, 128:] + gathered_out[h, :, 128:] * fade
+
+    slots = placed.shape[0]
+    cap = slots // sp
+    width = stream.shape[1]
+
+    def prepare_routing():
+        for copy in routing:
+            copy.wait()
+        lanes = lax.broadcasted_iota(jnp.int32, (sp, tok_rows), 0)
+        matches = [(lanes == ids[j : j + 1, :]).astype(f32) for j in range(TOP)]
+        order = (tok_rows, tok_rows)
+        before = lax.broadcasted_iota(jnp.int32, order, 0) < lax.broadcasted_iota(jnp.int32, order, 1)
+        named = functools.reduce(lambda a, b: a + b, matches)
+        earlier = jnp.dot(named.astype(bf16), before.astype(bf16), preferred_element_type=f32)
+        slot_rows = lax.broadcasted_iota(jnp.int32, (slots, tok_rows), 0)
+        either = None
+        for j in range(TOP):
+            rank = jnp.sum(matches[j] * earlier, axis=0, keepdims=True).astype(jnp.int32)
+            earlier = earlier + matches[j]
+            chosen = jnp.where(slot_rows == ids[j : j + 1, :] * cap + rank, 1.0, 0.0)
+            hot[j] = chosen.T.astype(bf16)
+            mix_column[j] = jnp.broadcast_to(mix[j : j + 1, :], order).T
+            either = chosen if either is None else either + chosen
+        select[...] = either.astype(bf16)
+
+    def columns(owner):
+        return pl.ds(pl.multiple_of(owner * width, width), width)
+
+    def arrival(place, sem):
+        return pltpu.make_async_copy(place, place, sem)
+
+    own_columns = columns(tp_id)
+
+    def block(index):
+        return pl.ds(pl.multiple_of(index * cap, cap), cap)
+
+    def ends(target_level, q):
+        return 2 * target_level + flip(core, q)
+
+    def handoff(k, q, target_level):
+        return remote(
+            placed.at[block(ends(target_level, q)), :],
+            rows_in.at[level, pl.ds(q * cap, cap), own_columns],
+            z_send.at[k, q],
+            z_recv.at[level, q],
+            ends(target_level, q),
+            tp_id,
+        )
+
+    parts = {0: (0, 0, 0), 1: (1, 0, 0), 2: (0, 0, 1), 3: (1, 0, 1), 4: (0, 1, 1), 5: (1, 1, 0)}
+
+    def pass_on(k, slot):
+        q, borrowed, to_far = parts[slot]
+        owner = tp_id
+        if borrowed:
+            owner = near if slot == 4 else far
+        place = rows_in.at[k, pl.ds(q * cap, cap), columns(owner)]
+        target = far if to_far else near
+        return remote(place, place, t_send.at[k, slot], t_recv.at[k, slot], sp_id, target)
+
+    def open_chunk(k):
+        @pl.when(level != k)
+        def _():
+            arrival(rows_in.at[k, pl.ds(0, cap), own_columns], z_recv.at[k, 0]).wait()
+
+        pass_on(k, 0).start()
+        pass_on(k, 2).start()
+        arrival(rows_in.at[k, pl.ds(cap, cap), own_columns], z_recv.at[k, 1]).wait()
+        pass_on(k, 3).start()
+        pass_on(k, 1).start()
+
+    def relay(k):
+        pass_on(k, 0).wait_recv()
+        pass_on(k, 4).start()
+        pass_on(k, 3).wait_recv()
+        pass_on(k, 5).start()
+
+    def push(k, slot):
+        src, target = {
+            0: (part.at[k, pl.ds(0, cap), columns(near)], near),
+            1: (part.at[k, pl.ds(0, cap), columns(across)], near),
+            2: (part.at[k, pl.ds(cap, cap), columns(far)], far),
+            3: (part.at[k, pl.ds(cap, cap), columns(across)], far),
+            4: (turned.at[k, 0], far),
+            5: (turned.at[k, 1], near),
+        }[slot]
+        return remote(src, landed.at[k, slot], r_send.at[k, slot], r_recv.at[k, slot], sp_id, target)
+
+    def wide(value):
+        return value.astype(f32)
+
+    def turn(k):
+        push(k, 1).wait_recv()
+        turned[k, 0] = (wide(part[k, :cap, columns(far)]) + wide(landed[k, 1])).astype(bf16)
+        push(k, 4).start()
+        push(k, 3).wait_recv()
+        turned[k, 1] = (wide(part[k, cap:, columns(near)]) + wide(landed[k, 3])).astype(bf16)
+        push(k, 5).start()
+
+    def back(k, q):
+        return remote(
+            summed.at[k, q],
+            returned.at[block(sp_id), :],
+            y_send.at[k, q],
+            y_recv.at[level, q],
+            ends(k, q),
+            tp_id,
+        )
+
+    def close(k):
+        for q in range(2):
+            push(k, 2 * q).wait_recv()
+            push(k, 4 + q).wait_recv()
+            value = wide(part[k, q * cap : q * cap + cap, own_columns])
+            value = (value + wide(landed[k, 2 * q]) + wide(landed[k, 4 + q])).astype(bf16)
+            summed[k, q] = value
+            if q == 1:
+                back(k, q).start()
+                continue
+
+            @pl.when(level == k)
+            def _():
+                returned[block(sp_id), :] = summed[k, 0]
+
+            @pl.when(level != k)
+            def _():
+                back(k, 0).start()
+
+    actions = {"open": open_chunk, "relay": relay, "turn": turn, "close": close}
+
+    def run(point):
+        for here, plan in enumerate(plans(chips)):
+            events = plan.get(point, ())
+            if events:
+
+                @pl.when(level == here)
+                def _():
+                    for action, k in events:
+                        actions[action](k)
+
+    def forward(d):
+        @pl.when(level >= d)
+        def _():
+            arrival(blocks.at[d, 0, own_quarter, :], l_recv.at[d]).wait()
+            for slot in range(3):
+                spread(d, slot).start()
+
+    for d in range(1, chips // 2):
+        forward(d)
+    share(0).wait_recv()
+    project(0)
+    for d in range(chips // 2, chips - 1):
+        forward(d)
+    attend(0)
+    forward(chips - 1)
+    prepare_routing()
+    for d in range(1, chips):
+
+        @pl.when(level >= d)
+        def _():
+            for slot in range(3):
+                spread(d, slot).wait_recv()
+            share(d).start()
+
+    run("gathered")
+    for d in range(1, chips):
+        if d == chips - 1:
+            run("last")
+
+        @pl.when(level >= d)
+        def _():
+            share(d).wait_recv()
+            project(d)
+            attend(d)
+
+    def share_of(h):
+        return gathered_out[h, :, :128] / gathered_out[h, :, 128:]
+
+    for h in range(heads_major):
+        mixed[:, h * 128 : h * 128 + 128] = share_of(h).astype(bf16)
+    for tile in range(-(-heads_minor // pack)):
+        result = None
+        for member in range(min(pack, heads_minor - tile * pack)):
+            h = heads_major + tile * pack + member
+            value = share_of(h)
+            result = value if result is None else jnp.where(lane < member * NOPE_MINOR, result, value)
+        first = (heads_major + tile) * 128
+        mixed[:, first : first + 128] = result.astype(bf16)
+
+    for copy in late:
+        copy.wait()
+
+    mid = tok_rows // 2
+    mids = (pl.ds(0, mid), pl.ds(mid, mid))
+    rows = mixed[...]
+    spread_started = []
+
+    def fill_out(owner):
+        spread_part[:, columns(owner)] = jnp.dot(rows, projection[:, columns(owner)], preferred_element_type=f32).astype(bf16)
+
+    def push_out(src, slot, target):
+        copy = remote(src, spread_landed.at[slot], o_send.at[slot], o_recv.at[slot], sp_id, target)
+        copy.start()
+        spread_started.append(copy)
+        return copy
+
+    fill_out(across)
+    second = push_out(spread_part.at[mids[0], columns(across)], 1, near)
+    fourth = push_out(spread_part.at[mids[1], columns(across)], 3, far)
+    fill_out(near)
+    first = push_out(spread_part.at[mids[0], columns(near)], 0, near)
+    fill_out(far)
+    third = push_out(spread_part.at[mids[1], columns(far)], 2, far)
+    fill_out(tp_id)
+    second.wait_recv()
+    spread_turned[0] = (spread_part[mids[0], columns(far)].astype(f32) + spread_landed[1].astype(f32)).astype(bf16)
+    fifth = push_out(spread_turned.at[0], 4, far)
+    fourth.wait_recv()
+    spread_turned[1] = (spread_part[mids[1], columns(near)].astype(f32) + spread_landed[3].astype(f32)).astype(bf16)
+    sixth = push_out(spread_turned.at[1], 5, near)
+    run("pushed")
+    for q, plain, bent in ((0, first, fifth), (1, third, sixth)):
+        plain.wait_recv()
+        value = spread_part[mids[q], columns(tp_id)].astype(f32) + residual[mids[q], :].astype(f32)
+        value = value + spread_landed[2 * q].astype(f32)
+        bent.wait_recv()
+        stream[mids[q], :] = (value + spread_landed[4 + q].astype(f32)).astype(bf16)
+
+    units = gate.shape[1]
+    placed[...] = jnp.dot(select[...], stream[...], preferred_element_type=f32).astype(bf16)
+
+    handoff(0, 1, level).start()
+    for k in range(chips - 1, 0, -1):
+        for q in range(2):
+            handoff(k, q, flip(level, k)).start()
+    rows_in[level, 0:cap, own_columns] = placed[block(sp_id), :]
+
+    def ready(k):
+        for slot in (1, 2, 4, 5):
+            pass_on(k, slot).wait_recv()
+        rows = rows_in[k].astype(f32)
+        power = jnp.mean(rows * rows, axis=1, keepdims=True)
+        normed[...] = (rows * lax.rsqrt(power + norm_eps) * gain[...]).astype(bf16)
+
+    def expand():
+        tile = 256
+        rows = normed[...]
+        for first in range(0, units, tile):
+            span = slice(first, first + tile)
+            gate_pre = jnp.dot(rows, gate[:, span], preferred_element_type=f32)
+            up_pre = jnp.dot(rows, up[:, span], preferred_element_type=f32)
+            hidden[:, span] = (gate_pre / (1.0 + jnp.exp(-gate_pre)) * up_pre).astype(bf16)
+
+    def contract(k):
+        rows = hidden[...]
+
+        def fill(owner):
+            part[k, :, columns(owner)] = jnp.dot(
+                rows, down[:, columns(owner)], preferred_element_type=f32
+            ).astype(bf16)
+
+        fill(across)
+        push(k, 1).start()
+        push(k, 3).start()
+        fill(near)
+        push(k, 0).start()
+        fill(far)
+        push(k, 2).start()
+        fill(tp_id)
+
+    run("streamed")
+    for copy in expert_loads:
+        copy.wait()
+    for k in range(chips):
+        ready(k)
+        expand()
+        run(f"between {k}")
+        contract(k)
+        run(f"after {k}")
+
+    for k in range(chips):
+        for q in range(2):
+            if q == 1:
+                arrival(returned.at[block(ends(k, q)), :], y_recv.at[k, q]).wait()
+                continue
+
+            @pl.when(level != k)
+            def _():
+                arrival(returned.at[block(ends(k, q)), :], y_recv.at[k, q]).wait()
+
+    total = stream[...].astype(f32)
+    for j in range(TOP):
+        total = total + jnp.dot(hot[j], returned[...], preferred_element_type=f32) * mix_column[j][:, :1]
+    out_ref[...] = total.astype(bf16)
+    for k in range(chips):
+        for slot in range(6):
+            pass_on(k, slot).wait_send()
+            push(k, slot).wait_send()
+        back(k, 1).wait_send()
+
+        @pl.when(level != k)
+        def _():
+            back(k, 0).wait_send()
+
+        for q in range(2):
+            if k > 0 or q > 0:
+                handoff(k, q, flip(level, k)).wait_send()
+    for copy in spread_started:
+        copy.wait_send()
+    share(0).wait_send()
+    for d in range(1, chips):
+
+        @pl.when(level + d < chips)
+        def _():
+            lift(d).wait_send()
+
+        @pl.when(level >= d)
+        def _():
+            share(d).wait_send()
+            for slot in range(3):
+                spread(d, slot).wait_send()
+
+
+def fused_layer(
+    sp,
+    tp,
+    query_major,
+    query_minor,
+    latent_rows,
+    rope_keys,
+    key_up_major,
+    value_up_major,
+    key_up_minor,
+    value_up_minor,
+    out_major,
+    out_minor,
+    residual,
+    norm_gain,
+    expert_ids,
+    expert_weights,
+    gate_proj,
+    up_proj,
+    down_proj,
+):
+    tok_rows, latent = latent_rows.shape
+    rope_width = rope_keys.shape[1]
+    width = residual.shape[1]
+    features = tp * width
+    units = gate_proj.shape[2]
+    chips = sp // 2
+    cap = 2 * tok_rows * TOP // sp
+    slots = sp * cap
+    heads = (key_up_major.shape[1] // NOPE_MAJOR, key_up_minor.shape[1] // NOPE_MINOR)
+    count = heads[0] + heads[1]
+    joined = latent + rope_width + -(latent + rope_width) % 128
+    kept = key_up_major.shape[1] + key_up_minor.shape[1] + value_up_major.shape[1] + value_up_minor.shape[1]
+    mixed = value_up_major.shape[1] + value_up_minor.shape[1]
+    dma = pltpu.SemaphoreType.DMA
+    bf16, f32 = jnp.bfloat16, jnp.float32
+    table = jnp.asarray(rope_table(sp * tok_rows, rope_width))
+    operands = (
+        query_major,
+        query_minor,
+        latent_rows,
+        rope_keys.T,
+        table,
+        key_up_major,
+        value_up_major,
+        key_up_minor,
+        value_up_minor,
+        out_major,
+        out_minor,
+        residual,
+        expert_ids.T,
+        expert_weights.T,
+        norm_gain.reshape(1, -1),
+        gate_proj,
+        up_proj,
+        down_proj,
+    )
+    vmem = pltpu.VMEM
+    return pl.pallas_call(
+        functools.partial(layer_kernel, sp, heads),
+        out_shape=jax.ShapeDtypeStruct((tok_rows, width), bf16),
+        in_specs=[pl.BlockSpec(memory_space=pl.ANY)] * len(operands),
+        out_specs=pl.BlockSpec(memory_space=pltpu.VMEM),
+        scratch_shapes=[
+            vmem(query_major.shape, bf16),
+            vmem(query_minor.shape, bf16),
+            vmem((rope_width, tok_rows), bf16),
+            vmem((tok_rows, 2 * rope_width), f32),
+            vmem((latent, kept), bf16),
+            vmem((mixed, features), bf16),
+            vmem(residual.shape, bf16),
+            vmem((TOP, tok_rows), jnp.int32),
+            vmem((TOP, tok_rows), f32),
+            vmem((1, features), f32),
+            vmem((features, units), bf16),
+            vmem((features, units), bf16),
+            vmem((units, features), bf16),
+            vmem((chips, 2, tok_rows, joined), bf16),
+            vmem((count, tok_rows, 256), bf16),
+            vmem((2 * tok_rows, kept), bf16),
+            vmem((count, tok_rows, 128), f32),
+            vmem((count, tok_rows, 2 * tok_rows), f32),
+            vmem((count, tok_rows, 2 * tok_rows), bf16),
+            vmem((count, tok_rows, 128), f32),
+            vmem((count, tok_rows, 256), f32),
+            vmem((tok_rows, mixed), bf16),
+            vmem((tok_rows, features), bf16),
+            vmem((6, tok_rows // 2, width), bf16),
+            vmem((2, tok_rows // 2, width), bf16),
+            vmem((tok_rows, width), bf16),
+            vmem((slots, tok_rows), bf16),
+            vmem((TOP, tok_rows, slots), bf16),
+            vmem((TOP, tok_rows, tok_rows), f32),
+            vmem((slots, width), bf16),
+            vmem((chips, 2 * cap, features), bf16),
+            vmem((2 * cap, features), bf16),
+            vmem((2 * cap, units), bf16),
+            vmem((chips, 2 * cap, features), bf16),
+            vmem((chips, 6, cap, width), bf16),
+            vmem((chips, 2, cap, width), bf16),
+            vmem((chips, 2, cap, width), bf16),
+            vmem((slots, width), bf16),
+            dma((len(operands),)),
+            dma((3, 4)),
+            dma((chips,)),
+            dma((chips,)),
+            dma((chips, 3)),
+            dma((chips, 3)),
+            dma((chips,)),
+            dma((chips,)),
+            dma((6,)),
+            dma((6,)),
+            dma((chips, 2)),
+            dma((chips, 2)),
+            dma((chips, 6)),
+            dma((chips, 6)),
+            dma((chips, 6)),
+            dma((chips, 6)),
+            dma((chips, 2)),
+            dma((chips, 2)),
+        ],
+        compiler_params=pltpu.CompilerParams(
+            collective_id=4, has_side_effects=True, vmem_limit_bytes=60 * 1024 * 1024
+        ),
+    )(*operands)
+
+
 def run_experts(rows, gain, gate_proj, up_proj, down_proj):
     slots, features = rows.shape
     units = gate_proj.shape[2]
@@ -551,6 +1326,31 @@
     down_proj,
 ):
     tok_rows = query_major.shape[0]
+    fast = tp == 4 and sp & (sp - 1) == 0
+    fast = fast and tok_rows % 64 == 0 and (2 * tok_rows * TOP // sp) % 16 == 0
+    fast = fast and key_up_major.shape[1] % 128 == 0 and key_up_minor.shape[1] % 128 == 0
+    if fast:
+        return fused_layer(
+            sp,
+            tp,
+            query_major,
+            query_minor,
+            latent_rows,
+            rope_keys,
+            key_up_major,
+            value_up_major,
+            key_up_minor,
+            value_up_minor,
+            out_major,
+            out_minor,
+            residual,
+            norm_gain,
+            expert_ids,
+            expert_weights,
+            gate_proj,
+            up_proj,
+            down_proj,
+        )
     row_start = lax.axis_index("sp") * tok_rows
     positions = row_start + jnp.arange(tok_rows, dtype=jnp.int32)
     rope_width = rope_keys.shape[1]

time: 123 us -> 76.2 us (0.62)
  the two profiles are of different devices: /device:TPU:0 before, /device:TPU:25 now
where the time goes in v3:
time: 76.2 us; the launch traced here: 76 us
  Pallas kernels  74.5 us (98%)
  local copies, waits for them, and re-layouts  1.57 us (2%)
    pallas_call x1, Pallas kernels, fused_layer(): pl.pallas_call(functools.partial(layer_kernel, sp, heads), out_shape=jax....  74.5 us
    unnamed x1, local copies, waits for them, and re-layouts  1.57 us

profile of v3, /device:TPU:25, one launch (start us, length us, event | category | flops | bytes accessed | tf_op | source)
XLA Modules:
  0.0 76.0 jit_solution(14100174481020547824)
XLA Ops:
  0.0 74.5 %shard_map.172 = bf16[128,512]{1,0:T(8,128)(2,1)} custom-call(bf16[128,768]{1,0:T(8,128)(2,1)} %q_major_ref.1, bf16[128,512]{1,0:T(8,128)(2,1)} %q_minor_ref.1, bf16[128,512]{1,0:T(8,128)(2,1)} %latent_ref.1, bf16[64,128]{1,0:T(8,128)(2,1)} %bitcast.4, f32[1024,128]{1,0:T(8,128)} %constant.2.clone.table_ref, bf16[512,512]{1,0:T(8,128)(2,1)} %key_major_ref.1, ...), custom_call_target="tpu_custom_call" | custom-call | tf_op jit(solution)/shard_map/pallas_call | solution.py:1210
  74.5 1.6 %copy.20 = bf16[128,512]{1,0:T(8,128)(2,1)} copy(bf16[128,512]{1,0:T(8,128)(2,1)} %shard_map.172) | data formatting | bytes 262144

commit v4 on v3

--- a/solution.py
+++ b/solution.py
@@ -529,36 +529,43 @@
     simple[f"after {last}"] += [("turn", last)] + [("close", k) for k in range(chips)]
     if chips != 4:
         return [simple] * chips
-    low = {
-        "streamed": [("open", 0), ("relay", 0)],
-        "between 0": [("open", 1)],
-        "after 0": [("relay", 1), ("open", 2)],
-        "between 1": [("relay", 2)],
-        "after 1": [("turn", 0)],
-        "between 2": [("open", 3)],
-        "after 2": [("relay", 3), ("turn", 1), ("close", 0), ("turn", 2), ("close", 1)],
-        "after 3": [("close", 2), ("turn", 3), ("close", 3)],
-    }
-    early = {
-        "pushed": [("open", 0)],
-    }
     ending = {
         "after 2": [("turn", 1), ("close", 0)],
         "after 3": [("turn", 2), ("close", 1), ("turn", 3), ("close", 2), ("close", 3)],
     }
+    bottom = {
+        "streamed": [("open", 0), ("relay", 0)],
+        "between 0": [("open", 1)],
+        "after 0": [("relay", 1)],
+        "between 1": [("open", 2)],
+        "after 1": [("relay", 2), ("open", 3), ("turn", 0)],
+        "between 2": [("relay", 3)],
+    }
+    lower = {
+        "streamed": [("open", 0), ("open", 1), ("relay", 0)],
+        "between 0": [("relay", 1), ("open", 2)],
+        "between 1": [("relay", 2)],
+        "after 1": [("open", 3), ("turn", 0)],
+        "between 2": [("relay", 3)],
+    }
     upper = {
-        "streamed": [("relay", 0), ("open", 1), ("open", 2), ("relay", 1)],
-        "between 0": [("relay", 2)],
+        "pushed": [("open", 0)],
+        "streamed": [("relay", 0), ("open", 1), ("open", 2)],
+        "between 0": [("relay", 1)],
+        "after 0": [("relay", 2)],
         "between 1": [("open", 3)],
-        "after 1": [("relay", 3), ("turn", 0)],
+        "after 1": [("turn", 0)],
+        "between 2": [("relay", 3)],
     }
     top = {
-        "streamed": [("relay", 0), ("open", 3), ("open", 1), ("relay", 1), ("open", 2)],
-        "between 0": [("relay", 2)],
+        "pushed": [("open", 0)],
+        "streamed": [("relay", 0), ("open", 1), ("open", 3), ("open", 2)],
+        "between 0": [("relay", 1)],
         "after 0": [("relay", 3)],
+        "between 1": [("relay", 2)],
         "after 1": [("turn", 0)],
     }
-    return [low, low, early | upper | ending, early | top | ending]
+    return [bottom | ending, lower | ending, upper | ending, top | ending]
 
 
 def layer_kernel(
@@ -746,15 +753,13 @@
 
     for copy in asked:
         copy.wait()
-    expert_loads = []
-    pieces = expert_sem.shape[1]
+    pieces = 4
     for index, (src, dst) in enumerate(((gate_ref, gate), (up_ref, up), (down_ref, down))):
         count = dst.shape[0] // pieces
         for piece in range(pieces):
             span = pl.ds(piece * count, count)
-            copy = pltpu.make_async_copy(src.at[0, span, :], dst.at[span, :], expert_sem.at[index, piece])
+            copy = pltpu.make_async_copy(src.at[0, span, :], dst.at[span, :], expert_sem.at[index])
             copy.start()
-            expert_loads.append(copy)
     def column(ref, index):
         return ref[:, index * 128 : index * 128 + 128].astype(f32)
 
@@ -869,7 +874,7 @@
         return remote(
             placed.at[block(ends(target_level, q)), :],
             rows_in.at[level, pl.ds(q * cap, cap), own_columns],
-            z_send.at[k, q],
+            z_send,
             z_recv.at[level, q],
             ends(target_level, q),
             tp_id,
@@ -884,7 +889,7 @@
             owner = near if slot == 4 else far
         place = rows_in.at[k, pl.ds(q * cap, cap), columns(owner)]
         target = far if to_far else near
-        return remote(place, place, t_send.at[k, slot], t_recv.at[k, slot], sp_id, target)
+        return remote(place, place, t_send, t_recv.at[k, slot], sp_id, target)
 
     def open_chunk(k):
         @pl.when(level != k)
@@ -912,7 +917,7 @@
             4: (turned.at[k, 0], far),
             5: (turned.at[k, 1], near),
         }[slot]
-        return remote(src, landed.at[k, slot], r_send.at[k, slot], r_recv.at[k, slot], sp_id, target)
+        return remote(src, landed.at[k, slot], r_send, r_recv.at[k, slot], sp_id, target)
 
     def wide(value):
         return value.astype(f32)
@@ -929,7 +934,7 @@
         return remote(
             summed.at[k, q],
             returned.at[block(sp_id), :],
-            y_send.at[k, q],
+            y_send,
             y_recv.at[level, q],
             ends(k, q),
             tp_id,
@@ -981,25 +986,27 @@
         forward(d)
     attend(0)
     forward(chips - 1)
-    prepare_routing()
-    for d in range(1, chips):
-
+    def collect(d):
         @pl.when(level >= d)
         def _():
             for slot in range(3):
                 spread(d, slot).wait_recv()
             share(d).start()
 
-    run("gathered")
-    for d in range(1, chips):
-        if d == chips - 1:
-            run("last")
-
+    def process(d):
         @pl.when(level >= d)
         def _():
             share(d).wait_recv()
             project(d)
             attend(d)
+
+    collect(1)
+    prepare_routing()
+    process(1)
+    for d in range(2, chips):
+        collect(d)
+    for d in range(2, chips):
+        process(d)
 
     def share_of(h):
         return gathered_out[h, :, :128] / gathered_out[h, :, 128:]
@@ -1021,15 +1028,13 @@
     mid = tok_rows // 2
     mids = (pl.ds(0, mid), pl.ds(mid, mid))
     rows = mixed[...]
-    spread_started = []
 
     def fill_out(owner):
         spread_part[:, columns(owner)] = jnp.dot(rows, projection[:, columns(owner)], preferred_element_type=f32).astype(bf16)
 
     def push_out(src, slot, target):
-        copy = remote(src, spread_landed.at[slot], o_send.at[slot], o_recv.at[slot], sp_id, target)
+        copy = remote(src, spread_landed.at[slot], o_send, o_recv.at[slot], sp_id, target)
         copy.start()
-        spread_started.append(copy)
         return copy
 
     fill_out(across)
@@ -1058,9 +1063,19 @@
     placed[...] = jnp.dot(select[...], stream[...], preferred_element_type=f32).astype(bf16)
 
     handoff(0, 1, level).start()
-    for k in range(chips - 1, 0, -1):
-        for q in range(2):
-            handoff(k, q, flip(level, k)).start()
+
+    @pl.when(level == 0)
+    def _():
+        for k in range(1, chips):
+            for q in range(2):
+                handoff(k, q, flip(level, k)).start()
+
+    @pl.when(level > 0)
+    def _():
+        for k in range(chips - 1, 0, -1):
+            for q in range(2):
+                handoff(k, q, flip(level, k)).start()
+
     rows_in[level, 0:cap, own_columns] = placed[block(sp_id), :]
 
     def ready(k):
@@ -1097,8 +1112,8 @@
         fill(tp_id)
 
     run("streamed")
-    for copy in expert_loads:
-        copy.wait()
+    for index, ref in enumerate((gate, up, down)):
+        arrival(ref, expert_sem.at[index]).wait()
     for k in range(chips):
         ready(k)
         expand()
@@ -1106,35 +1121,23 @@
         contract(k)
         run(f"after {k}")
 
+    total = stream[...].astype(f32)
     for k in range(chips):
-        for q in range(2):
-            if q == 1:
-                arrival(returned.at[block(ends(k, q)), :], y_recv.at[k, q]).wait()
-                continue
-
-            @pl.when(level != k)
-            def _():
-                arrival(returned.at[block(ends(k, q)), :], y_recv.at[k, q]).wait()
-
-    total = stream[...].astype(f32)
-    for j in range(TOP):
-        total = total + jnp.dot(hot[j], returned[...], preferred_element_type=f32) * mix_column[j][:, :1]
-    out_ref[...] = total.astype(bf16)
-    for k in range(chips):
-        for slot in range(6):
-            pass_on(k, slot).wait_send()
-            push(k, slot).wait_send()
-        back(k, 1).wait_send()
-
-        @pl.when(level != k)
-        def _():
-            back(k, 0).wait_send()
-
+        source = flip(level, k)
         for q in range(2):
             if k > 0 or q > 0:
-                handoff(k, q, flip(level, k)).wait_send()
-    for copy in spread_started:
-        copy.wait_send()
+                arrival(returned.at[block(ends(source, q)), :], y_recv.at[source, q]).wait()
+        span = pl.ds(pl.multiple_of(source * 2 * cap, 2 * cap), 2 * cap)
+        for j in range(TOP):
+            picked = jnp.dot(hot[j, :, span], returned[span, :], preferred_element_type=f32)
+            total = total + picked * mix_column[j][:, :1]
+    out_ref[...] = total
+    arrival(landed, t_send).wait()
+    arrival(landed, r_send).wait()
+    sent = pl.ds(0, (sp - 1) * cap)
+    arrival(returned.at[sent, :], z_send).wait()
+    arrival(returned.at[sent, :], y_send).wait()
+    arrival(spread_landed, o_send).wait()
     share(0).wait_send()
     for d in range(1, chips):
 
@@ -1209,7 +1212,7 @@
     vmem = pltpu.VMEM
     return pl.pallas_call(
         functools.partial(layer_kernel, sp, heads),
-        out_shape=jax.ShapeDtypeStruct((tok_rows, width), bf16),
+        out_shape=pltpu.VMEM((tok_rows, width), f32),
         in_specs=[pl.BlockSpec(memory_space=pl.ANY)] * len(operands),
         out_specs=pl.BlockSpec(memory_space=pltpu.VMEM),
         scratch_shapes=[
@@ -1252,28 +1255,28 @@
             vmem((chips, 2, cap, width), bf16),
             vmem((slots, width), bf16),
             dma((len(operands),)),
-            dma((3, 4)),
+            dma((3,)),
             dma((chips,)),
             dma((chips,)),
             dma((chips, 3)),
             dma((chips, 3)),
             dma((chips,)),
             dma((chips,)),
+            dma,
             dma((6,)),
-            dma((6,)),
+            dma,
             dma((chips, 2)),
-            dma((chips, 2)),
+            dma,
             dma((chips, 6)),
+            dma,
             dma((chips, 6)),
-            dma((chips, 6)),
-            dma((chips, 6)),
-            dma((chips, 2)),
+            dma,
             dma((chips, 2)),
         ],
         compiler_params=pltpu.CompilerParams(
             collective_id=4, has_side_effects=True, vmem_limit_bytes=60 * 1024 * 1024
         ),
-    )(*operands)
+    )(*operands).astype(bf16)
 
 
 def run_experts(rows, gain, gate_proj, up_proj, down_proj):

time: 76.2 us -> 72.7 us (0.954)
  Pallas kernels: 74.5 us -> 71.9 us
  local copies, waits for them, and re-layouts: 1.57 us -> 0 us
    pallas_call x1, Pallas kernels: 74.5 us -> 71.9 us  [fused_layer(): pl.pallas_call(functools.partial(layer_kernel, sp, heads), out_shape=pltp...]
    unnamed x1 -> x0, local copies, waits for them, and re-layouts: 1.57 us -> none
where the time goes in v4:
time: 72.7 us; the launch traced here: 72.6 us
  Pallas kernels  71.9 us (99%)
    pallas_call x1, Pallas kernels, fused_layer(): pl.pallas_call(functools.partial(layer_kernel, sp, heads), out_shape=pltp...  71.9 us

profile of v4, /device:TPU:25, one launch (start us, length us, event | category | flops | bytes accessed | tf_op | source)
XLA Modules:
  0.0 72.6 jit_solution(14393027309440222918)
XLA Ops:
  0.0 71.9 %shard_map.172 = f32[128,512]{1,0:T(8,128)S(1)} custom-call(bf16[128,768]{1,0:T(8,128)(2,1)} %q_major_ref.1, bf16[128,512]{1,0:T(8,128)(2,1)} %q_minor_ref.1, bf16[128,512]{1,0:T(8,128)(2,1)} %latent_ref.1, bf16[64,128]{1,0:T(8,128)(2,1)} %bitcast.4, f32[1024,128]{1,0:T(8,128)} %constant.2.clone.table_ref, bf16[512,512]{1,0:T(8,128)(2,1)} %key_major_ref.1, ...), custom_call_target="tpu_custom_call" | custom-call | tf_op jit(solution)/shard_map/pallas_call | solution.py:1213
  71.9 0.7 convert_element_type.3

commit v5 on v4

--- a/solution.py
+++ b/solution.py
@@ -519,6 +519,12 @@
     return np.concatenate([cosine, cosine, -sine, sine], axis=1).astype(np.float32)
 
 
+def orders(chips):
+    if chips != 4:
+        return [tuple(range(chips))] * chips
+    return [(0, 1, 2, 3), (0, 1, 2, 3), (0, 1, 3, 2), (0, 1, 2, 3)]
+
+
 def plans(chips):
     last = chips - 1
     simple = {"streamed": [("open", 0), ("relay", 0)]}
@@ -530,42 +536,52 @@
     if chips != 4:
         return [simple] * chips
     ending = {
-        "after 2": [("turn", 1), ("close", 0)],
-        "after 3": [("turn", 2), ("close", 1), ("turn", 3), ("close", 2), ("close", 3)],
+        "between 3": [("turn", 2)],
+        "after 3": [("send", 1), ("close", 2), ("turn", 3), ("close", 3), ("turn", 1), ("close", 1)],
     }
     bottom = {
         "streamed": [("open", 0), ("relay", 0)],
         "between 0": [("open", 1)],
-        "after 0": [("relay", 1)],
-        "between 1": [("open", 2)],
-        "after 1": [("relay", 2), ("open", 3), ("turn", 0)],
-        "between 2": [("relay", 3)],
+        "after 0": [("relay", 1), ("turn", 0)],
+        "between 1": [("close", 0), ("open", 2)],
+        "after 1": [("open", 3), ("relay", 2)],
+        "between 2": [("relay", 3), ("turn", 1)],
+        "after 2": [("close", 1)],
+        "between 3": [("turn", 2)],
+        "after 3": [("close", 2), ("turn", 3), ("close", 3)],
     }
     lower = {
         "streamed": [("open", 0), ("open", 1), ("relay", 0)],
         "between 0": [("relay", 1), ("open", 2)],
-        "between 1": [("relay", 2)],
-        "after 1": [("open", 3), ("turn", 0)],
+        "between 1": [("open", 3), ("relay", 2), ("turn", 0)],
         "between 2": [("relay", 3)],
+        "after 2": [("close", 0)],
     }
     upper = {
         "pushed": [("open", 0)],
         "streamed": [("relay", 0), ("open", 1), ("open", 2)],
         "between 0": [("relay", 1)],
         "after 0": [("relay", 2)],
-        "between 1": [("open", 3)],
-        "after 1": [("turn", 0)],
-        "between 2": [("relay", 3)],
+        "between 1": [("open", 3), ("turn", 0)],
+        "after 1": [("relay", 3), ("close", 0)],
+        "between 2": [("turn", 1)],
+        "after 2": [("close", 1)],
+        "between 3": [("turn", 3)],
+        "after 3": [("close", 3), ("turn", 2), ("close", 2)],
     }
     top = {
         "pushed": [("open", 0)],
         "streamed": [("relay", 0), ("open", 1), ("open", 3), ("open", 2)],
         "between 0": [("relay", 1)],
         "after 0": [("relay", 3)],
-        "between 1": [("relay", 2)],
-        "after 1": [("turn", 0)],
+        "between 1": [("relay", 2), ("turn", 0)],
+        "after 1": [("close", 0)],
+        "between 2": [("turn", 1)],
+        "after 2": [("close", 1)],
+        "between 3": [("turn", 2)],
+        "after 3": [("close", 2), ("turn", 3), ("close", 3)],
     }
-    return [bottom | ending, lower | ending, upper | ending, top | ending]
+    return [bottom, lower | ending, upper, top]
 
 
 def layer_kernel(
@@ -785,12 +801,10 @@
     log2e = 1.4426950408889634
     contract = (((1,), (1,)), ((), ()))
 
-    def project(d):
-        for q in range(2):
-            rows = blocks[d, q, :, :latent]
-            kept[pl.ds(q * tok_rows, tok_rows), :] = jnp.dot(rows, weights[...], preferred_element_type=f32).astype(
-                bf16
-            )
+    def project(d, q):
+        span = pl.ds(q * tok_rows, tok_rows)
+        rows = blocks[d, q, :, :latent]
+        kept[d, span, :] = jnp.dot(rows, weights[...], preferred_element_type=f32).astype(bf16)
 
     everyone = range(heads_major + heads_minor)
 
@@ -802,7 +816,7 @@
         for h in everyone:
             nope = NOPE_MAJOR if h < heads_major else NOPE_MINOR
             key_at = tile_of(h) * 128 + (0 if h < heads_major else spans[1].start)
-            key = jnp.concatenate([kept[:, key_at : key_at + 128], tails], axis=1)
+            key = jnp.concatenate([kept[d, :, key_at : key_at + 128], tails], axis=1)
             scale = (nope + rope_width) ** (-0.5) * log2e
             value = lax.dot_general(queries[h], key, contract, preferred_element_type=f32) * scale
             if d == 0:
@@ -823,7 +837,7 @@
         ones = jnp.ones((keys, 128), bf16)
         for h in everyone:
             value_at = tile_of(h) * 128 + (spans[2].start if h < heads_major else spans[3].start)
-            value = jnp.concatenate([kept[:, value_at : value_at + 128], ones], axis=1)
+            value = jnp.concatenate([kept[d, :, value_at : value_at + 128], ones], axis=1)
             summed = jnp.dot(chances[h], value, preferred_element_type=f32)
             if d == 0:
                 gathered_out[h] = summed
@@ -959,7 +973,11 @@
             def _():
                 back(k, 0).start()
 
-    actions = {"open": open_chunk, "relay": relay, "turn": turn, "close": close}
+    def send(k):
+        for slot in (1, 3, 0, 2):
+            push(k, slot).start()
+
+    actions = {"send": send, "open": open_chunk, "relay": relay, "turn": turn, "close": close}
 
     def run(point):
         for here, plan in enumerate(plans(chips)):
@@ -980,8 +998,9 @@
 
     for d in range(1, chips // 2):
         forward(d)
+    project(0, 0)
     share(0).wait_recv()
-    project(0)
+    project(0, 1)
     for d in range(chips // 2, chips - 1):
         forward(d)
     attend(0)
@@ -992,12 +1011,13 @@
             for slot in range(3):
                 spread(d, slot).wait_recv()
             share(d).start()
+            project(d, 0)
 
     def process(d):
         @pl.when(level >= d)
         def _():
             share(d).wait_recv()
-            project(d)
+            project(d, 1)
             attend(d)
 
     collect(1)
@@ -1064,18 +1084,9 @@
 
     handoff(0, 1, level).start()
 
-    @pl.when(level == 0)
-    def _():
-        for k in range(1, chips):
-            for q in range(2):
-                handoff(k, q, flip(level, k)).start()
-
-    @pl.when(level > 0)
-    def _():
-        for k in range(chips - 1, 0, -1):
-            for q in range(2):
-                handoff(k, q, flip(level, k)).start()
-
+    for k in range(chips - 1, 0, -1):
+        for q in range(2):
+            handoff(k, q, flip(level, k)).start()
     rows_in[level, 0:cap, own_columns] = placed[block(sp_id), :]
 
     def ready(k):
@@ -1094,7 +1105,7 @@
             up_pre = jnp.dot(rows, up[:, span], preferred_element_type=f32)
             hidden[:, span] = (gate_pre / (1.0 + jnp.exp(-gate_pre)) * up_pre).astype(bf16)
 
-    def contract(k):
+    def contract(k, late):
         rows = hidden[...]
 
         def fill(owner):
@@ -1102,24 +1113,37 @@
                 rows, down[:, columns(owner)], preferred_element_type=f32
             ).astype(bf16)
 
+        def leave(*chosen):
+            def start():
+                for slot in chosen:
+                    push(k, slot).start()
+
+            if late:
+                pl.when(level != 1)(start)
+            else:
+                start()
+
         fill(across)
-        push(k, 1).start()
-        push(k, 3).start()
+        leave(1, 3)
         fill(near)
-        push(k, 0).start()
+        leave(0)
         fill(far)
-        push(k, 2).start()
+        leave(2)
         fill(tp_id)
 
     run("streamed")
     for index, ref in enumerate((gate, up, down)):
         arrival(ref, expert_sem.at[index]).wait()
-    for k in range(chips):
+    choices = orders(chips)
+    for step in range(chips):
+        k = choices[0][step]
+        for here in range(1, chips):
+            k = jnp.where(level == here, choices[here][step], k)
         ready(k)
         expand()
-        run(f"between {k}")
-        contract(k)
-        run(f"after {k}")
+        run(f"between {step}")
+        contract(k, chips == 4 and step == 1)
+        run(f"after {step}")
 
     total = stream[...].astype(f32)
     for k in range(chips):
@@ -1231,7 +1255,7 @@
             vmem((units, features), bf16),
             vmem((chips, 2, tok_rows, joined), bf16),
             vmem((count, tok_rows, 256), bf16),
-            vmem((2 * tok_rows, kept), bf16),
+            vmem((chips, 2 * tok_rows, kept), bf16),
             vmem((count, tok_rows, 128), f32),
             vmem((count, tok_rows, 2 * tok_rows), f32),
             vmem((count, tok_rows, 2 * tok_rows), bf16),

time: 72.7 us -> 70.2 us (0.966)
  Pallas kernels: 71.9 us -> 69.3 us
    pallas_call x1, Pallas kernels: 71.9 us -> 69.3 us  [fused_layer(): pl.pallas_call(functools.partial(layer_kernel, sp, heads), out_shape=pltp...]
where the time goes in v5:
time: 70.2 us; the launch traced here: 70 us
  Pallas kernels  69.3 us (99%)
    pallas_call x1, Pallas kernels, fused_layer(): pl.pallas_call(functools.partial(layer_kernel, sp, heads), out_shape=pltp...  69.3 us

profile of v5, /device:TPU:25, one launch (start us, length us, event | category | flops | bytes accessed | tf_op | source)
XLA Modules:
  0.0 70.0 jit_solution(6969050623068097091)
XLA Ops:
  0.0 69.3 %shard_map.172 = f32[128,512]{1,0:T(8,128)S(1)} custom-call(bf16[128,768]{1,0:T(8,128)(2,1)} %q_major_ref.1, bf16[128,512]{1,0:T(8,128)(2,1)} %q_minor_ref.1, bf16[128,512]{1,0:T(8,128)(2,1)} %latent_ref.1, bf16[64,128]{1,0:T(8,128)(2,1)} %bitcast.4, f32[1024,128]{1,0:T(8,128)} %constant.2.clone.table_ref, bf16[512,512]{1,0:T(8,128)(2,1)} %key_major_ref.1, ...), custom_call_target="tpu_custom_call" | custom-call | tf_op jit(solution)/shard_map/pallas_call | solution.py:1237
  69.3 0.7 convert_element_type.3
